TPU v7x, 512 devices: a whole 4x4x16 slice. The times are simulated.
512 devices in a mesh: dp: 4 (over x), kv: 64 (over z, y), tp: 2 (over core).
Axes of the slice: x: 4, y: 4, z: 16, core: 2. Of those that a mesh axis runs over, the one named last changes fastest.
Arguments:
- tokens: bfloat16 [768, 2048], P('dp', ('kv', 'tp')), may hold values from -21 to 21
- state: float32 [768, 8, 128, 128], P(('dp', 'kv'), 'tp'), may hold values from -3 to 3
- mix_gain: bfloat16 [2048], P(('kv', 'tp')), may hold values from 0.099609375 to 1.8984375
- w_query: bfloat16 [2048, 1024], P('kv', 'tp'), may hold values from -0.125 to 0.125
- w_key: bfloat16 [2048, 1024], P('kv', 'tp'), may hold values from -0.125 to 0.125
- w_value: bfloat16 [2048, 1024], P('kv', 'tp'), may hold values from -0.125 to 0.125
- w_beta: bfloat16 [2048, 8], P('kv', 'tp'), may hold values from -0.125 to 0.125
- w_decay: bfloat16 [2048, 8], P('kv', 'tp'), may hold values from -0.125 to 0.125
- decay_log: float32 [8], P('tp'), may hold values from -1.5 to 1
- head_gain: bfloat16 [128], replicated, may hold values from 0.099609375 to 1.8984375
- w_out: bfloat16 [1024, 2048], P('tp', 'kv'), may hold values from -0.1875 to 0.1875
- ff_gain: bfloat16 [2048], P(('kv', 'tp')), may hold values from 0.099609375 to 1.8984375
- w_up: bfloat16 [2048, 8192], P(None, ('kv', 'tp')), may hold values from -0.125 to 0.125
- w_down: bfloat16 [8192, 2048], P(('kv', 'tp')), may hold values from -0.25 to 0.25
Outputs:
- output: bfloat16 [768, 2048], P('dp', ('kv', 'tp'))
- new_state: float32 [768, 8, 128, 128], P(('dp', 'kv'), 'tp')
All inputs are finite; a program needn't handle non-finite values.
Results may differ from a plain program's by a relative error of at most 0.013.
Values may be sent and summed in bfloat16 or wider, within the bound.
A program may use at most 64 MiB of HBM per device.

v0:
```python
import math

import jax
import jax.numpy as jnp
from jax import lax
from jax.sharding import PartitionSpec as P

D = 2048


def gather_turned(arrays, axis, dims):
    turned = [jnp.moveaxis(a, dim, 0) for a, dim in zip(arrays, dims)]
    both = jnp.concatenate([t.reshape(len(t), -1) for t in turned], axis=1)
    filled, at, finished = (lax.all_gather(both, axis, axis=0, tiled=True), 0, [])
    for t, dim in zip(turned, dims):
        slab = filled[:, at : at + t[0].size].reshape(-1, *t.shape[1:])
        finished.append(jnp.moveaxis(slab, 0, dim))
        at += t[0].size
    return tuple(finished)


def in_blocks(value, dim, size):
    before, after = (value.shape[:dim], value.shape[dim + 1 :])
    return jnp.moveaxis(value.reshape(*before, size, -1, *after), dim, 0)


def sent_and_summed(value, axis, dim):
    size = lax.axis_size(axis)
    pieces = lax.all_to_all(in_blocks(value, dim, size), axis, 0, 0, tiled=True)
    return jnp.sum(pieces.astype(jnp.float32), axis=0)


def in_one_piece(arrays, axis, dim, along):
    widths = [math.prod(a.shape[along:]) for a in arrays]
    both = jnp.concatenate(
        [a.reshape(*a.shape[:along], w) for a, w in zip(arrays, widths)], axis=along
    )
    filled = sent_and_summed(both, axis, dim)
    pieces = jnp.split(filled, [sum(widths[:k]) for k in range(1, len(widths))], axis=along)
    return tuple(
        (b.reshape(*filled.shape[:along], *a.shape[along:]) for a, b in zip(arrays, pieces))
    )


def copy_for_each(value, axis):
    copies = jnp.broadcast_to(value, (lax.axis_size(axis), *value.shape))
    return lax.all_to_all(copies, axis, split_axis=0, concat_axis=0, tiled=True)


def in_order(pieces, dim):
    pieces = jnp.moveaxis(pieces, 0, dim)
    shape = pieces.shape
    return pieces.reshape(*shape[:dim], shape[dim] * shape[dim + 1], *shape[dim + 2 :])


def collect(value, axis, dim):
    pieces = copy_for_each(value, axis)
    return in_order(pieces, dim)


def one_gather(arrays, axis, dims):
    vector = jnp.concatenate([a.reshape(-1) for a in arrays])
    lines, at, finished = (lax.all_gather(vector, axis), 0, [])
    for a, dim in zip(arrays, dims):
        pieces = lines[:, at : at + a.size].reshape(-1, *a.shape)
        finished.append(in_order(pieces, dim))
        at += a.size
    return tuple(finished)


def local(
    tokens,
    state,
    mix_gain,
    w_query,
    w_key,
    w_value,
    w_beta,
    w_decay,
    decay_log,
    head_gain,
    w_out,
    ff_gain,
    w_up,
    w_down,
):
    seq_count = state.shape[0]
    heads_local = state.shape[1]
    head_size = state.shape[2]
    tokens_wide, gain_wide = gather_turned((tokens, mix_gain[None, :]), "tp", (1, 1))
    wide_float = tokens_wide.astype(jnp.float32)
    scaled = (wide_float * gain_wide.astype(jnp.float32)).astype(jnp.bfloat16)
    query_part = jnp.dot(scaled, w_query, preferred_element_type=jnp.float32)
    key_part = jnp.dot(scaled, w_key, preferred_element_type=jnp.float32)
    value_part = jnp.dot(scaled, w_value, preferred_element_type=jnp.float32)
    gate_part = jnp.concatenate(
        [
            jnp.dot(scaled, w_beta, preferred_element_type=jnp.float32),
            jnp.dot(scaled, w_decay, preferred_element_type=jnp.float32),
        ],
        axis=1,
    )
    square_part = jnp.sum(wide_float * wide_float, axis=1)
    query_sum, key_sum, value_sum, gate_sum, square_sum = in_one_piece(
        (
            query_part.astype(jnp.bfloat16),
            key_part.astype(jnp.bfloat16),
            value_part.astype(jnp.bfloat16),
            gate_part.astype(jnp.bfloat16),
            square_part.astype(jnp.bfloat16),
        ),
        "kv",
        0,
        1,
    )
    inverse = lax.rsqrt(square_sum / D + 1e-06)[:, None]
    query = (inverse * query_sum).reshape(seq_count, heads_local, head_size)
    key_rows = (inverse * key_sum).reshape(seq_count, heads_local, head_size)
    value = (inverse * value_sum).reshape(seq_count, heads_local, head_size)
    gates = inverse * gate_sum
    beta = jax.nn.sigmoid(gates[:, :heads_local])
    decay = -jnp.exp(decay_log)[None, :] * jax.nn.softplus(gates[:, heads_local:])
    qnorm = query * lax.rsqrt(jnp.sum(query * query, axis=-1, keepdims=True) + 1e-06)
    knorm = key_rows * lax.rsqrt(jnp.sum(key_rows * key_rows, axis=-1, keepdims=True) + 1e-06)
    kept = state * jnp.exp(decay)[:, :, None, None]
    predicted = jnp.sum(kept * knorm[:, :, :, None], axis=2)
    new_state = (
        kept + (beta[:, :, None] * knorm)[:, :, :, None] * (value - predicted)[:, :, None, :]
    )
    heads = jnp.sum(new_state * qnorm[:, :, :, None], axis=2) / jnp.sqrt(jnp.float32(head_size))
    normed = (
        heads
        * lax.rsqrt(jnp.mean(heads * heads, axis=-1, keepdims=True) + 1e-06)
        * head_gain.astype(jnp.float32)
    )
    normed = normed.astype(jnp.bfloat16).reshape(seq_count, heads_local * head_size)
    partial_mix = jnp.dot(collect(normed, "kv", 0), w_out, preferred_element_type=jnp.float32)
    mixed = sent_and_summed(partial_mix.astype(jnp.bfloat16), "tp", 1)
    resid = (tokens.astype(jnp.float32) + mixed).astype(jnp.bfloat16)
    up_weight, down_weight, gain_pair = one_gather(
        (w_up, w_down, ff_gain[None, :]), "tp", (1, 0, 1)
    )
    gain_local = gain_pair[0]
    work_rows = lax.all_to_all(resid, "tp", split_axis=0, concat_axis=1, tiled=True)
    resid_float = work_rows.astype(jnp.float32)
    whole_rows, whole_gain = gather_turned((work_rows, gain_local[None, :]), "kv", (1, 1))
    whole_float = whole_rows.astype(jnp.float32)
    inverse2 = lax.rsqrt(jnp.mean(whole_float * whole_float, axis=1, keepdims=True) + 1e-06)
    scaled2 = (whole_float * whole_gain.astype(jnp.float32)).astype(jnp.bfloat16)
    up_rows = jnp.dot(scaled2, up_weight, preferred_element_type=jnp.float32) * inverse2
    act = jnp.square(jax.nn.relu(up_rows)).astype(jnp.bfloat16)
    summed = sent_and_summed(
        lax.dot_general(
            down_weight, act, (((0,), (1,)), ((), ())), preferred_element_type=jnp.float32
        ).astype(jnp.bfloat16),
        "kv",
        0,
    )
    results = (resid_float + summed.T).astype(jnp.bfloat16)
    output = results
    output = lax.all_to_all(output, "tp", split_axis=1, concat_axis=0, tiled=True)
    return (output, new_state)


def solution(mesh):
    placed = (
        P("dp", ("kv", "tp")),
        P(("dp", "kv"), "tp", None, None),
        P(("kv", "tp")),
        P("kv", "tp"),
        P("kv", "tp"),
        P("kv", "tp"),
        P("kv", "tp"),
        P("kv", "tp"),
        P("tp"),
        P(),
        P("tp", "kv"),
        P(("kv", "tp")),
        P(None, ("kv", "tp")),
        P(("kv", "tp"), None),
    )
    return jax.shard_map(
        local,
        mesh=mesh,
        in_specs=placed,
        out_specs=(P("dp", ("kv", "tp")), P(("dp", "kv"), "tp", None, None)),
        check_vma=False,
    )
```

profile of v0, /device:TPU:1, one launch (start us, length us, event | category | flops | bytes accessed | tf_op | source)
XLA Modules:
  0.0 285.4 jit_solution(2601442207486391683)
XLA Ops:
  7.2 0.8 copy.104
  7.9 0.8 pad_maximum_fusion.1
  8.7 8.3 %all_gather.12 = bf16[32,193]{1,0:T(8,128)(2,1)S(1)} all-gather(bf16[16,193]{1,0:T(8,128)(2,1)S(1)} %pad_maximum_fusion.1), channel_id=1, replica_groups=mesh['dp'=4,'kv'=64,'tp'=2] {'tp'}, dimensions={0}, use_global_device_ids=true | all-gather | bytes 18528 | tf_op jit(solution)/shard_map/all_gather | solution.py:14
  17.0 0.2 convert_reduce_fusion.4
  17.2 0.3 convolution_convert_fusion.3
  17.6 0.1 concatenate.28
  17.7 1.1 convolution_convert_fusion.2
  18.7 0.1 concatenate.29
  18.9 0.3 convolution_convert_fusion.1
  19.2 0.1 concatenate.30
  19.3 0.2 convolution_convert_fusion.6
  19.5 0.2 concatenate.31
  19.7 0.5 copy.105
  20.2 0.2 convolution_convert_fusion.5
  20.4 0.2 concatenate.32
  20.6 0.5 copy.106
  21.1 0.2 convert_element_type.127
  21.3 2.0 concatenate.33
  23.3 13.2 %all-to-all-start = ((bf16[64,3,1545]{2,1,0:T(4,128)(2,1)}), bf16[64,3,1545]{2,1,0:T(4,128)(2,1)S(1)}, u32[]{:S(2)}, u32[]{:S(2)}) async-start(bf16[64,3,1545]{2,1,0:T(4,128)(2,1)} %concatenate.33), calls=%async_computation | async-start | bytes 1703936 | tf_op jit(solution)/shard_map/all_to_all | solution.py:29
  36.7 0.3 copy.115
  37.0 0.3 reshape.146
  37.3 1.3 dynamic-slice
  39.3 4.9 %dynamic-update-slice = bf16[524320]{0:T(1024)(128)(2,1)S(1)} dynamic-update-slice(bf16[524320]{0:T(1024)(128)(2,1)S(1)} %broadcast.84, bf16[262160]{0:T(1024)(128)(2,1)S(1)} %pad_maximum_fusion, u32[]{:T(128)} %bitcast.7) | dynamic-update-slice | bytes 1048644
  44.2 1.0 copy-done.1
  45.2 43.0 %all-reduce.3.cloned.1.call-done = bf16[524320]{0:T(1024)(128)(2,1)} async-done(((bf16[524320]{0:T(1024)(128)(2,1)}), bf16[524320]{0:T(1024)(128)(2,1)}) %all-reduce.3.cloned.1.call-update) | async-done | bytes 1048656
  88.2 2.6 reshape.153
  90.9 0.4 convert_reduce_fusion
  91.2 0.2 fusion.21
  91.6 0.1 multiply_reduce_fusion.4
  91.7 0.1 copy.120
  91.8 0.1 copy.109
  91.9 0.1 multiply_reduce_fusion.3
  92.0 0.1 copy.121
  92.1 0.1 copy.111
  92.2 0.1 fusion.18
  92.3 0.1 broadcast_multiply_fusion.2
  92.4 0.3 multiply_reduce_fusion.1
  92.7 1.4 multiply_reduce_fusion
  94.1 0.1 multiply_reduce_fusion.2
  94.2 0.1 copy.112
  94.3 0.1 copy.113
  94.5 0.8 broadcast_in_dim.2
  95.2 14.4 %all-to-all-start.1 = ((bf16[64,3,512]{2,1,0:T(4,128)(2,1)}), bf16[64,3,512]{2,1,0:T(4,128)(2,1)S(1)}, u32[]{:S(2)}, u32[]{:S(2)}) async-start(bf16[64,3,512]{2,1,0:T(4,128)(2,1)} %broadcast_in_dim.2), calls=%async_computation.1 | async-start | bytes 524288 | tf_op jit(solution)/shard_map/all_to_all | solution.py:47
  109.6 0.7 fusion.28
  110.3 0.5 reshape_reshape.3
  110.8 0.7 reshape.148
  111.5 0.3 copy.117
  111.9 0.3 slice-done
  112.2 0.1 transpose_broadcast_in_dim_squeeze_reshape_transpose_reshape.4
  112.2 17.7 %all-to-all-done.1 = bf16[64,3,512]{2,1,0:T(4,128)(2,1)S(1)} async-done(((bf16[64,3,512]{2,1,0:T(4,128)(2,1)}), bf16[64,3,512]{2,1,0:T(4,128)(2,1)S(1)}, u32[]{:S(2)}, u32[]{:S(2)}) %all-to-all-start.1) | async-done | bytes 196640 | tf_op jit(solution)/shard_map/all_to_all | solution.py:47
  130.0 0.2 reshape.144
  130.2 0.1 convolution_convert_fusion.4
  130.3 6.5 %all_to_all.58 = bf16[2,192,16]{1,2,0:T(8,128)(2,1)S(1)} all-to-all(bf16[2,192,16]{1,2,0:T(8,128)(2,1)S(1)} %bitcast.54), channel_id=1, replica_groups=mesh['dp'=4,'kv'=64,'tp'=2] {'tp'}, dimensions={0} | all-to-all | bytes 24576 | tf_op jit(solution)/shard_map/all_to_all | solution.py:29
  136.8 0.1 all_to_all.43
  136.9 3.7 %all_to_all.59 = bf16[2,96,16]{1,2,0:T(8,128)(2,1)S(1)} all-to-all(bf16[2,96,16]{1,2,0:T(8,128)(2,1)S(1)} %copy.114), channel_id=1, replica_groups=mesh['dp'=4,'kv'=64,'tp'=2] {'tp'}, dimensions={0} | all-to-all | bytes 12288 | tf_op jit(solution)/shard_map/all_to_all | solution.py:144
  140.7 72.8 %all_gather.15 = bf16[2048,97]{1,0:T(8,128)(2,1)S(1)} all-gather(bf16[32,97]{1,0:T(8,128)(2,1)S(1)} %pad_maximum_fusion.2), channel_id=1, replica_groups=mesh['dp'=4,'kv'=64,'tp'=2] {'kv'}, dimensions={0}, use_global_device_ids=true | all-gather | bytes 403520 | tf_op jit(solution)/shard_map/all_gather | solution.py:14
  213.5 0.4 convert_reduce_fusion.1
  213.9 0.3 fusion.4
  214.2 1.1 convolution_convert_fusion
  215.3 0.3 copy.118
  215.6 27.9 %all_to_all.60 = bf16[64,32,96]{2,1,0:T(8,128)(2,1)S(1)} all-to-all(bf16[64,32,96]{2,1,0:T(8,128)(2,1)S(1)} %bitcast.50), channel_id=1, replica_groups=mesh['dp'=4,'kv'=64,'tp'=2] {'kv'}, dimensions={0} | all-to-all | bytes 786432 | tf_op jit(solution)/shard_map/all_to_all | solution.py:29
  243.4 0.1 convert_reduce_fusion.2
  243.6 34.2 %all_to_all.61 = bf16[96,2,16]{0,2,1:T(8,128)(2,1)S(1)} all-to-all(bf16[96,2,16]{0,2,1:T(8,128)(2,1)S(1)} %bitcast.57), channel_id=1, replica_groups=mesh['dp'=4,'kv'=64,'tp'=2] {'tp'}, dimensions={1} | all-to-all | bytes 12288 | tf_op jit(solution)/shard_map/all_to_all | solution.py:161
  277.8 0.7 all_to_all.51
  (56 shorter events, 0.8 us)
Async XLA Ops:
  7.2 10.1 %copy-start = (bf16[32,512]{1,0:T(8,128)(2,1)S(1)}, bf16[32,512]{1,0:T(8,128)(2,1)}, u32[]{:S(2)}) copy-start(bf16[32,512]{1,0:T(8,128)(2,1)} %param.17) | copy-start | bytes 98308
  7.2 11.7 %copy-start.6 = (bf16[32,512]{1,0:T(8,128)(2,1)S(1)}, bf16[32,512]{1,0:T(8,128)(2,1)}, u32[]{:S(2)}) copy-start(bf16[32,512]{1,0:T(8,128)(2,1)} %param.19) | copy-start | bytes 98308
  17.2 2.1 copy-start.10
  17.5 2.6 copy-start.11
  23.3 13.3 %copy-start.5 = (bf16[64,2048]{1,0:T(8,128)(2,1)S(1)}, bf16[64,2048]{1,0:T(8,128)(2,1)}, u32[]{:S(2)}) copy-start(bf16[64,2048]{1,0:T(8,128)(2,1)} %param.27) | copy-start | bytes 786436
  23.3 13.4 %copy-start.4 = (bf16[2048,64]{0,1:T(8,128)(2,1)S(1)}, bf16[2048,64]{0,1:T(8,128)(2,1)}, u32[]{:S(2)}) copy-start(bf16[2048,64]{0,1:T(8,128)(2,1)} %param.26) | copy-start | bytes 786436
  23.3 67.6 %all-to-all-start = ((bf16[64,3,1545]{2,1,0:T(4,128)(2,1)}), bf16[64,3,1545]{2,1,0:T(4,128)(2,1)S(1)}, u32[]{:S(2)}, u32[]{:S(2)}) async-start(bf16[64,3,1545]{2,1,0:T(4,128)(2,1)} %concatenate.33), calls=%async_computation | async-start | bytes 1703936 | tf_op jit(solution)/shard_map/all_to_all | solution.py:29
  36.5 0.7 copy-start.9
  36.6 51.7 %all-reduce.3.cloned.1.call-start = ((), (), s32[]{:S(2)}) async-start(), calls=%async_computation.6 | async-start | bytes 2101248
  39.3 5.9 %copy-start.12 = (bf16[128]{0:T(256)(128)(2,1)S(1)}, bf16[128]{0:T(256)(128)(2,1)}, u32[]{:S(2)}) copy-start(bf16[128]{0:T(256)(128)(2,1)} %param.23) | copy-start | bytes 772
  39.3 5.9 %copy-start.13 = (f32[4]{0:T(128)S(1)}, f32[4]{0:T(128)}, u32[]{:S(2)}) copy-start(f32[4]{0:T(128)} %param.22) | copy-start | bytes 52
  44.2 1.0 copy-start.1
  90.8 19.5 %copy-start.2 = (bf16[2,262160]{1,0:T(2,128)(2,1)}, bf16[2,262160]{1,0:T(2,128)(2,1)S(1)}, u32[]{:S(2)}) copy-start(bf16[2,262160]{1,0:T(2,128)(2,1)S(1)} %reshape.153) | copy-start | bytes 3145924
  90.8 1.6 copy-start.3
  95.2 34.7 %all-to-all-start.1 = ((bf16[64,3,512]{2,1,0:T(4,128)(2,1)}), bf16[64,3,512]{2,1,0:T(4,128)(2,1)S(1)}, u32[]{:S(2)}, u32[]{:S(2)}) async-start(bf16[64,3,512]{2,1,0:T(4,128)(2,1)} %broadcast_in_dim.2), calls=%async_computation.1 | async-start | bytes 524288 | tf_op jit(solution)/shard_map/all_to_all | solution.py:47
  111.5 0.7 slice-start
  111.5 18.7 %copy-start.7 = (bf16[512,32]{0,1:T(8,128)(2,1)S(1)}, bf16[512,32]{0,1:T(8,128)(2,1)}, u32[]{:S(2)}) copy-start(bf16[512,32]{0,1:T(8,128)(2,1)} %param.24) | copy-start | bytes 98308
  111.5 25.3 %copy-start.8 = (bf16[192,16]{0,1:T(8,128)(2,1)S(1)}, bf16[192,16]{0,1:T(8,128)(2,1)}, u32[]{:S(2)}) copy-start(bf16[192,16]{0,1:T(8,128)(2,1)} %param.14) | copy-start | bytes 18436
Sparse Core Ops, SparseCore 0:
  45.3 42.8 all-reduce.2
where the time goes:
time: 286 us; the launch traced here: 285 us
  blocking collectives  153 us (53%)
  waiting for transfers between devices  60.7 us (21%)
  starting transfers between devices  27.6 us (10%)
  local copies, waits for them, and re-layouts  20.3 us (7%)
  between operations  15.1 us (5%)
  other arithmetic  4.86 us (2%)
  matrix products  3.28 us (1%)
    all_gather x2, blocking collectives, gather_turned(): lax.all_gather(both, axis, axis=0, tiled=True)  81.1 us
    unnamed x2, waiting for transfers between devices  43 us
    all_to_all x2, blocking collectives, sent_and_summed(): pieces = lax.all_to_all(in_blocks(value, dim, size), axis, 0, 0, tiled=True)  34.3 us
    all_to_all x1, blocking collectives, local(): lax.all_to_all(output, 'tp', split_axis=1, concat_axis=0, tiled=True)  34.2 us
    all_to_all x1, waiting for transfers between devices, copy_for_each(): return lax.all_to_all(copies, axis, split_axis=0, concat_axis=0, tiled=True)  17.7 us
    all_to_all x1, starting transfers between devices, copy_for_each(): return lax.all_to_all(copies, axis, split_axis=0, concat_axis=0, tiled=True)  14.4 us
    all_to_all x1, starting transfers between devices, sent_and_summed(): pieces = lax.all_to_all(in_blocks(value, dim, size), axis, 0, 0, tiled=True)  13.2 us
    unnamed x35, local copies, waits for them, and re-layouts  7.79 us
  transfers between devices with their start and end apart: 3, of which 2 were waited for; matrix products, arithmetic and copies ran while one was open for 4% of the time, Pallas kernels for 0%

commit v1 on v0

v1 whole, which is shorter than its diff:
```python
import functools

import jax
import jax.numpy as jnp
from jax import lax
from jax.experimental import pallas as pl
from jax.experimental.pallas import tpu as pltpu
from jax.sharding import PartitionSpec as P

D = 2048
NZ = 16
NY = 4
MESH = pl.DeviceIdType.MESH
F32 = jnp.float32
BF16 = jnp.bfloat16
NT = (((1,), (1,)), ((), ()))
R1 = 40
R3 = 32


def iota(shape, dim):
    return lax.broadcasted_iota(jnp.int32, shape, dim)


def body(
    tile_hbm,
    state_hbm,
    wq_hbm,
    wk_hbm,
    wv_hbm,
    wo_hbm,
    wu_hbm,
    wd_hbm,
    head_gain_ref,
    decay_log_ref,
    out_ref,
    state_out,
    tbuf,
    wbuf,
    wo,
    fbuf,
    st,
    qbuf,
    xs,
    zs,
    zsend,
    zrecv,
    accs,
    g12,
    hs,
    nsend,
    nrecv,
    nf,
    rsend,
    rrecv,
    res,
    dsend,
    drecv,
    ysend,
    yrecv,
    lsem,
    ssem,
    rsem,
):
    kv = lax.axis_index("kv")
    tp = lax.axis_index("tp")
    z = kv // NY
    y = kv % NY
    me8 = y * 2 + tp
    half = z // 8

    barrier = pltpu.get_barrier_semaphore()

    def greet_z(j, carry):
        t = (z * 2 + tp + j) % (2 * NZ)
        pl.semaphore_signal(
            barrier, inc=1, device_id={"kv": (t // 2) * NY + y, "tp": t % 2}, device_id_type=MESH
        )
        return carry

    lax.fori_loop(1, 2 * NZ, greet_z, 0)

    def greet_y(j, carry):
        other = z * NY + (y + j) % NY
        for t in range(2):
            pl.semaphore_signal(
                barrier, inc=1, device_id={"kv": other, "tp": t}, device_id_type=MESH
            )
        return carry

    lax.fori_loop(1, NY, greet_y, 0)

    def local(src, dst, k):
        return pltpu.make_async_copy(src, dst, lsem.at[k])

    loads = [
        local(tile_hbm, tbuf.at[me8], 0),
        local(wq_hbm, wbuf.at[y, 0], 1),
        local(wk_hbm, wbuf.at[y, 1], 2),
        local(wv_hbm, wbuf.at[y, 2], 3),
        local(
            wo_hbm,
            wo.at[pl.ds(pl.multiple_of(y * 32, 32), 32), pl.ds(pl.multiple_of(tp * 512, 512), 512)],
            4,
        ),
        local(wu_hbm, fbuf.at[tp, y, 0], 5),
        local(wd_hbm, fbuf.at[tp, y, 1], 6),
        local(state_hbm, st, 7),
    ]
    for c in loads:
        c.start()

    src_row, seq_col = iota((1024, 256), 0), iota((1024, 256), 1)
    lane = src_row % 128
    place = 12 * ((src_row // 128 % 2) * 8 + lane % 8) + 3 * (src_row // 256) + lane // 8
    qbuf[...] = jnp.where((seq_col == place) & (lane < 24), 1.0, 0.0).astype(BF16)

    row, col = iota((56, 256), 0), iota((56, 256), 1)
    wanted = jnp.where(row < 48, 12 * (row % 16) + 3 * y + row // 16, row + 144)
    pick = jnp.where((col == wanted) & (row < 50), 1.0, 0.0).astype(BF16)

    er, ec = iota((512, 128), 0), iota((512, 128), 1)
    spread = jnp.where((ec == er // 128 * 32 + er % 128) & (er % 128 < 32), 1.0, 0.0).astype(BF16)

    for c in loads[:7]:
        c.wait()

    pl.semaphore_wait(barrier, 2 * NZ - 1 + 2 * (NY - 1))

    def push(src, dst, k, where):
        pltpu.make_async_remote_copy(
            src_ref=src,
            dst_ref=dst,
            send_sem=ssem.at[k],
            recv_sem=rsem.at[k],
            device_id=where,
            device_id_type=MESH,
        ).start()

    def to_eight(src_of, dst, k):
        def one(j, carry):
            p = (me8 + j) % 8
            push(src_of(p), dst, k, {"kv": z * NY + p // 2, "tp": p % 2})
            return carry

        lax.fori_loop(1, 8, one, 0)

    def to_column(ref, k):
        def one(j, carry):
            push(ref, ref, k, {"kv": z * NY + (y + j) % NY})
            return carry

        lax.fori_loop(1, NY, one, 0)

    def got(ref, sem):
        pltpu.make_async_copy(ref, ref, sem).wait()

    my_wo = wo.at[
        pl.ds(pl.multiple_of(y * 32, 32), 32), pl.ds(pl.multiple_of(tp * 512, 512), 512)
    ]
    to_eight(lambda p: tbuf.at[me8], tbuf.at[me8], 0)
    to_column(wbuf.at[y], 1)
    to_eight(lambda p: my_wo, my_wo, 2)
    to_column(fbuf.at[tp, y], 3)

    got(tbuf.at[pl.ds(0, 7)], rsem.at[0])
    tiles = tbuf[...]
    turned = tiles[:, :16, :].reshape(128, 256)
    chosen = lax.dot_general(pick, turned, NT, preferred_element_type=F32)
    xs[...] = chosen
    x = chosen[:48]
    scaled = (x * chosen[48:49]).astype(BF16)
    square = jnp.sum(x * x, axis=1, keepdims=True)
    square_hi = square.astype(BF16).astype(F32)
    own = jnp.concatenate([tbuf[2 * k + tp, 16:32, :128] for k in range(NY)], axis=1)
    gate_w = jnp.dot(own, spread, preferred_element_type=F32).astype(BF16)
    gate_w = jnp.concatenate([gate_w, jnp.zeros((112, 128), BF16)], axis=0)
    gate = lax.dot_general(scaled, gate_w, NT, preferred_element_type=F32)
    gl = iota((48, 128), 1)
    gate = jnp.where(gl == 8, square_hi, jnp.where(gl == 9, square - square_hi, gate))

    got(wbuf.at[pl.ds(0, 3)], rsem.at[1])
    for m in range(3):
        weight = wbuf[:, m].reshape(128, 512)
        part = jnp.dot(scaled, weight, preferred_element_type=F32)
        for h in range(4):
            for i in range(3):
                zs[pl.ds(m * 12 + h * 3 + i, NZ, R1), :] = part[
                    i * 16 : (i + 1) * 16, h * 128 : (h + 1) * 128
                ]
    for i in range(3):
        zs[pl.ds(36 + i, NZ, R1), :] = gate[i * 16 : (i + 1) * 16]
    zs[pl.ds(39, NZ, R1), :] = jnp.zeros((NZ, 128), F32)
    zsend[...] = zs[...].reshape(NZ, R1, 128).astype(BF16)

    def along(src_of, dst, k):
        def one(n, carry):
            d = NZ // 2 + ((n + 1) // 2) * (1 - 2 * (n % 2))
            far = (z + d) % NZ
            push(src_of(far), dst, k, {"kv": far * NY + y})
            return carry

        lax.fori_loop(0, NZ - 1, one, 0)

    along(lambda far: zsend.at[far], zrecv.at[z], 4)
    zrecv[z] = zsend[z]
    loads[7].wait()
    got(zrecv.at[pl.ds(0, NZ - 1)], rsem.at[4])

    acc = zrecv[0].astype(F32)
    for k in range(1, NZ):
        acc = acc + zrecv[k].astype(F32)
    accs[...] = acc
    for h in range(4):
        g12[3 * h : 3 * h + 3, :] = accs[36:39, :]
    g = g12[0:12, :]
    r12, l12 = iota((12, 128), 0), iota((12, 128), 1)
    head_of = r12 // 3

    def take(mask):
        return jnp.sum(jnp.where(mask, g, 0.0), axis=1, keepdims=True)

    inverse = lax.rsqrt(take((l12 == 8) | (l12 == 9)) / D + 1e-06)
    beta = jax.nn.sigmoid(inverse * take(l12 == head_of))
    u = inverse * take(l12 == head_of + 4)
    soft = jnp.maximum(u, 0.0) + jnp.log1p(jnp.exp(-jnp.abs(u)))
    h1 = iota((12, 1), 0) // 3
    rate = jnp.where(
        h1 == 0,
        decay_log_ref[0],
        jnp.where(h1 == 1, decay_log_ref[1], jnp.where(h1 == 2, decay_log_ref[2], decay_log_ref[3])),
    )
    keep = jnp.exp(-jnp.exp(rate) * soft)
    query = inverse * accs[0:12, :]
    key = inverse * accs[12:24, :]
    value = inverse * accs[24:36, :]
    qnorm = query * lax.rsqrt(jnp.sum(query * query, axis=1, keepdims=True) + 1e-06)
    knorm = key * lax.rsqrt(jnp.sum(key * key, axis=1, keepdims=True) + 1e-06)
    pad = jnp.zeros((104, 128), F32)
    g12[0:12, :] = qnorm
    g12[12:24, :] = knorm
    both = jnp.concatenate([g12[...], pad], axis=0).T
    for r in range(12):
        h, i = r // 3, r % 3
        kc = both[:, 12 + r : 13 + r]
        qc = both[:, r : r + 1]
        kept = st[i, h] * keep[r : r + 1, :]
        predicted = jnp.sum(kept * kc, axis=0, keepdims=True)
        new = kept + kc * (beta[r : r + 1, :] * (value[r : r + 1, :] - predicted))
        st[i, h] = new
        hs[r : r + 1, :] = jnp.sum(new * qc, axis=0, keepdims=True)
    heads = hs[...] / jnp.sqrt(jnp.float32(128))
    heads = jnp.where(iota((16, 128), 0) < 12, heads, 0.0)
    normed = (
        heads
        * lax.rsqrt(jnp.mean(heads * heads, axis=1, keepdims=True) + 1e-06)
        * head_gain_ref[...].astype(F32)
    )
    nsend[...] = normed.astype(BF16)
    state_copy = local(st, state_out, 8)
    state_copy.start()

    slot = (z % 8) * 2 + tp

    def spread_heads(n, carry):
        d = (NZ // 2 + ((n + 1) // 2) * (1 - 2 * (n % 2))) % NZ
        far = (z + d) % NZ
        push(nsend, nrecv.at[slot], 5, {"kv": far * NY + y, "tp": half})
        return carry

    lax.fori_loop(0, NZ - 1, spread_heads, 0)

    @pl.when(half == tp)
    def _():
        nrecv[slot] = nsend[...]
        got(nrecv.at[pl.ds(0, 15)], rsem.at[5])

    @pl.when(half != tp)
    def _():
        push(nsend, nrecv.at[slot], 5, {"tp": half})
        got(nrecv, rsem.at[5])

    got(wo.at[pl.ds(0, 112), :], rsem.at[2])
    nf[...] = nrecv[...].astype(F32).reshape(256, 128)
    wide = jnp.concatenate(
        [
            jnp.concatenate(
                [nf[pl.ds(t * 16 + h * 3 + i, 8, 32), :] for i in range(3)], axis=0
            )
            for t in range(2)
            for h in range(4)
        ],
        axis=1,
    ).astype(BF16)
    mixed = lax.dot_general(wide, wo[...], NT, preferred_element_type=F32)
    mine = jnp.concatenate(
        [xs[pl.ds(pl.multiple_of(i * 16 + tp * 8, 8), 8), :] for i in range(3)], axis=0
    )
    resid = (mine + mixed).astype(BF16).astype(F32)
    res[...] = resid
    scaled2 = (resid * xs[49:50, :]).astype(BF16).astype(F32)
    total = lax.dot_general(
        jnp.ones((8, 128), F32),
        jnp.concatenate([resid * resid, jnp.zeros((104, 128), F32)], axis=0),
        NT,
        preferred_element_type=F32,
        precision=lax.Precision.HIGHEST,
    )
    total_hi = total.astype(BF16).astype(F32)
    r8 = iota((8, 128), 0)
    tail = jnp.where(r8 == 0, total_hi, jnp.where(r8 == 1, total - total_hi, 0.0))
    rsend[...] = jnp.concatenate([scaled2, tail], axis=0).astype(BF16)
    along(lambda far: rsend, rrecv.at[z], 6)
    rrecv[z] = rsend[...]
    got(fbuf.at[tp, pl.ds(0, 3)], rsem.at[3])
    push(fbuf.at[tp], fbuf.at[tp], 7, {"tp": 1 - tp})
    got(rrecv.at[pl.ds(0, NZ - 1)], rsem.at[6])
    rows = jnp.concatenate([rrecv[k] for k in range(NZ)], axis=1)
    sums = rrecv[0, 16:32, :].astype(F32)
    for k in range(1, NZ):
        sums = sums + rrecv[k, 16:32, :].astype(F32)
    squares = sums[8:9] + sums[9:10]
    scale = lax.rsqrt(squares / D + 1e-06)
    dr, dc = iota((R3, 128), 0), iota((R3, 128), 1)
    scale = jnp.sum(jnp.where(dr == dc, scale, 0.0), axis=1, keepdims=True)
    got(fbuf.at[0], rsem.at[7])
    up_w = fbuf[:, :, 0].reshape(512, D)
    up = lax.dot_general(rows, up_w, NT, preferred_element_type=F32) * scale
    act = jnp.square(jnp.maximum(up, 0.0)).astype(BF16)
    for k in range(NZ // 2):
        part = jnp.dot(
            act,
            fbuf[:, :, 1, :, k * 256 : (k + 1) * 256].reshape(512, 256),
            preferred_element_type=F32,
        ).astype(BF16)
        dsend[2 * k] = part[:24, :128]
        dsend[2 * k + 1] = part[:24, 128:]
    along(lambda far: dsend.at[far], drecv.at[z], 8)
    drecv[z] = dsend[z]
    got(drecv.at[pl.ds(0, NZ - 1)], rsem.at[8])
    final = res[...]
    for k in range(NZ):
        final = final + drecv[k].astype(F32)
    final = jnp.concatenate([final, jnp.zeros((104, 128), F32)], axis=0).T
    ysend[...] = final.astype(BF16).reshape(8, 16, 128)
    to_eight(lambda p: ysend.at[p], yrecv.at[me8], 9)
    yrecv[me8] = ysend[me8]
    got(yrecv.at[pl.ds(0, 7)], rsem.at[9])
    pieces = jnp.concatenate([yrecv[k] for k in range(8)], axis=1)
    placed = jnp.dot(pieces, qbuf[...], preferred_element_type=F32)
    out_ref[...] = placed[:, :192].astype(BF16)

    state_copy.wait()
    got(tbuf.at[pl.ds(0, 7)], ssem.at[0])
    got(wbuf.at[pl.ds(0, 3)], ssem.at[1])
    got(wo.at[pl.ds(0, 112), :], ssem.at[2])
    got(fbuf.at[tp, pl.ds(0, 3)], ssem.at[3])
    got(zsend.at[pl.ds(0, NZ - 1)], ssem.at[4])

    @pl.when(half == tp)
    def _():
        got(nrecv.at[pl.ds(0, 15)], ssem.at[5])

    @pl.when(half != tp)
    def _():
        got(nrecv, ssem.at[5])

    got(rrecv.at[pl.ds(0, NZ - 1)], ssem.at[6])
    got(fbuf.at[tp], ssem.at[7])
    got(dsend.at[pl.ds(0, NZ - 1)], ssem.at[8])
    got(ysend.at[pl.ds(0, 7)], ssem.at[9])


def local_step(
    tokens,
    state,
    mix_gain,
    w_query,
    w_key,
    w_value,
    w_beta,
    w_decay,
    decay_log,
    head_gain,
    w_out,
    ff_gain,
    w_up,
    w_down,
):
    upper = jnp.concatenate(
        [tokens.T, mix_gain[:, None], ff_gain[:, None], jnp.zeros((16, 62), BF16)], axis=1
    )
    lower = jnp.concatenate([w_beta.T, w_decay.T], axis=0)
    tile = jnp.concatenate([upper, jnp.pad(lower, ((0, 8), (0, 224)))], axis=0)
    anywhere = pl.BlockSpec(memory_space=pltpu.HBM)
    vmem = pl.BlockSpec(memory_space=pltpu.VMEM)
    out, new_state = pl.pallas_call(
        body,
        name="layer",
        out_shape=(
            jax.ShapeDtypeStruct((16, 192), BF16),
            jax.ShapeDtypeStruct(state.shape, F32),
        ),
        in_specs=[anywhere] * 8 + [vmem, pl.BlockSpec(memory_space=pltpu.SMEM)],
        out_specs=(vmem, anywhere),
        scratch_shapes=[
            pltpu.VMEM((8, 32, 256), BF16),
            pltpu.VMEM((NY, 3, 32, 512), BF16),
            pltpu.VMEM((128, 1024), BF16),
            pltpu.VMEM((2, NY, 2, 64, D), BF16),
            pltpu.VMEM((3, 4, 128, 128), F32),
            pltpu.VMEM((1024, 256), BF16),
            pltpu.VMEM((56, 128), F32),
            pltpu.VMEM((NZ * R1, 128), F32),
            pltpu.VMEM((NZ, R1, 128), BF16),
            pltpu.VMEM((NZ, R1, 128), BF16),
            pltpu.VMEM((R1, 128), F32),
            pltpu.VMEM((24, 128), F32),
            pltpu.VMEM((16, 128), F32),
            pltpu.VMEM((16, 128), BF16),
            pltpu.VMEM((16, 16, 128), BF16),
            pltpu.VMEM((256, 128), F32),
            pltpu.VMEM((R3, 128), BF16),
            pltpu.VMEM((NZ, R3, 128), BF16),
            pltpu.VMEM((24, 128), F32),
            pltpu.VMEM((NZ, 24, 128), BF16),
            pltpu.VMEM((NZ, 24, 128), BF16),
            pltpu.VMEM((8, 16, 128), BF16),
            pltpu.VMEM((8, 16, 128), BF16),
            pltpu.SemaphoreType.DMA((9,)),
            pltpu.SemaphoreType.DMA((10,)),
            pltpu.SemaphoreType.DMA((10,)),
        ],
        compiler_params=pltpu.CompilerParams(
            collective_id=0, has_side_effects=True, vmem_limit_bytes=32 * 1024 * 1024
        ),
    )(
        tile,
        state,
        w_query,
        w_key,
        w_value,
        w_out.T,
        w_up.T,
        w_down,
        head_gain[None, :],
        decay_log,
    )
    return out.T, new_state


def solution(mesh):
    placed = (
        P("dp", ("kv", "tp")),
        P(("dp", "kv"), "tp", None, None),
        P(("kv", "tp")),
        P("kv", "tp"),
        P("kv", "tp"),
        P("kv", "tp"),
        P("kv", "tp"),
        P("kv", "tp"),
        P("tp"),
        P(),
        P("tp", "kv"),
        P(("kv", "tp")),
        P(None, ("kv", "tp")),
        P(("kv", "tp"), None),
    )
    return jax.shard_map(
        local_step,
        mesh=mesh,
        in_specs=placed,
        out_specs=(P("dp", ("kv", "tp")), P(("dp", "kv"), "tp", None, None)),
        check_vma=False,
    )
```

time: 286 us -> 75.3 us (0.26)
  blocking collectives: 153 us -> 0 us
  Pallas kernels: 0 us -> 66.6 us
  waiting for transfers between devices: 60.7 us -> 0 us
  starting transfers between devices: 27.6 us -> 0 us
  between operations: 15.1 us -> 0.73 us
  local copies, waits for them, and re-layouts: 20.3 us -> 7.43 us
  other arithmetic: 4.86 us -> 0.09 us
  matrix products: 3.28 us -> 0 us
    all_gather x2 -> x0, blocking collectives: 81.1 us -> none  [gather_turned(): lax.all_gather(both, axis, axis=0, tiled=True)]
    all_to_all x4 -> x0, blocking collectives: 72.3 us -> none  [the longest x2 34.3 us: sent_and_summed(): pieces = lax.all_to_all(in_blocks(value, dim, size), axis, 0, 0, tiled=True)]
    pallas_call x0 -> x1, Pallas kernels: none -> 66.6 us  [local_step(): pl.pallas_call(body, name='layer', out_shape=(jax.ShapeDtypeStruct((16, 1...]
    unnamed x2 -> x0, waiting for transfers between devices: 43 us -> none
    all_to_all x2 -> x0, starting transfers between devices: 27.6 us -> none  [the longest x1 14.4 us: copy_for_each(): return lax.all_to_all(copies, axis, split_axis=0, concat_axis=0, tiled=True)]
    all_to_all x2 -> x0, waiting for transfers between devices: 17.7 us -> none  [the longest x1 17.7 us: copy_for_each(): return lax.all_to_all(copies, axis, split_axis=0, concat_axis=0, tiled=True)]
    concatenate x8 -> x0, local copies, waits for them, and re-layouts: 3.68 us -> none  [the longest x4 2.34 us: in_one_piece(): jnp.concatenate([a.reshape(*a.shape[:along], w) for a, w in zip(arrays, w...]
    dot_general x7 -> x0, matrix products: 3.28 us -> none  [the longest x1 1.11 us: local(): lax.dot_general(down_weight, act, (((0,), (1,)), ((), ())), preferred_ele...]
  transfers between devices with their start and end apart: 3 -> 0, of which waited for: 2 -> 0; matrix products, arithmetic and copies ran while one was open for 4% -> 0% of each run, Pallas kernels for 0% -> 0%
where the time goes in v1:
time: 75.3 us; the launch traced here: 74.9 us
  Pallas kernels  66.6 us (88%)
  local copies, waits for them, and re-layouts  7.43 us (10%)
    pallas_call x1, Pallas kernels, local_step(): pl.pallas_call(body, name='layer', out_shape=(jax.ShapeDtypeStruct((16, 1...  66.6 us
    unnamed x30, local copies, waits for them, and re-layouts  7.24 us

profile of v1, /device:TPU:1, one launch (start us, length us, event | category | flops | bytes accessed | tf_op | source)
XLA Modules:
  0.0 74.9 jit_solution(16534625227701555919)
XLA Ops:
  0.6 0.0 copy-start.12
  0.6 0.0 copy-start.13
  0.7 0.0 copy-start.10
  0.7 0.0 copy-start.11
  0.7 0.0 copy-start.9
  0.7 0.6 copy-done.12
  1.3 0.0 copy-start.4
  1.3 0.1 copy.16
  1.4 0.0 copy-done.13
  1.4 0.0 copy-start.3
  1.4 0.1 copy.17
  1.5 0.0 copy-done.10
  1.5 0.0 copy-done.11
  1.5 0.0 copy-done.9
  1.5 0.0 copy-start.7
  1.5 0.0 copy-start.8
  1.6 0.1 pad_maximum_fusion.tile_hbm
  1.6 0.4 copy-done.4
  2.0 0.1 copy-done.3
  2.2 0.0 copy-done.7
  2.2 0.0 copy-done.8
  2.2 0.0 copy-start
  2.2 1.1 %copy-done = f32[3,4,128,128]{3,2,1,0:T(8,128)S(1)} copy-done((f32[3,4,128,128]{3,2,1,0:T(8,128)S(1)}, f32[3,4,128,128]{3,2,1,0:T(8,128)}, u32[]{:S(2)}) %copy-start) | copy-done | bytes 786456
  3.3 0.0 copy-start.1
  3.3 0.9 %copy-done.1 = bf16[2048,64]{0,1:T(8,128)(2,1)S(1)} copy-done((bf16[2048,64]{0,1:T(8,128)(2,1)S(1)}, bf16[2048,64]{0,1:T(8,128)(2,1)}, u32[]{:S(2)}) %copy-start.1) | copy-done | bytes 262168
  4.3 0.0 copy-start.2
  4.3 0.9 %copy-done.2 = bf16[64,2048]{1,0:T(8,128)(2,1)S(1)} copy-done((bf16[64,2048]{1,0:T(8,128)(2,1)S(1)}, bf16[64,2048]{1,0:T(8,128)(2,1)}, u32[]{:S(2)}) %copy-start.2) | copy-done | bytes 262168
  5.2 0.0 copy-start.5
  5.2 0.8 %copy-done.5 = bf16[32,512]{1,0:T(8,128)(2,1)S(1)} copy-done((bf16[32,512]{1,0:T(8,128)(2,1)S(1)}, bf16[32,512]{1,0:T(8,128)(2,1)}, u32[]{:S(2)}) %copy-start.5) | copy-done | bytes 32792
  6.0 0.0 copy-start.6
  6.0 0.8 %copy-done.6 = bf16[512,32]{0,1:T(8,128)(2,1)S(1)} copy-done((bf16[512,32]{0,1:T(8,128)(2,1)S(1)}, bf16[512,32]{0,1:T(8,128)(2,1)}, u32[]{:S(2)}) %copy-start.6) | copy-done | bytes 32792
  6.8 66.6 %layer.1 = (bf16[16,192]{1,0:T(8,128)(2,1)S(1)}, f32[3,4,128,128]{3,2,1,0:T(8,128)S(1)}) custom-call(bf16[32,256]{1,0:T(8,128)(2,1)S(1)} %pad_maximum_fusion.tile_hbm, f32[3,4,128,128]{3,2,1,0:T(8,128)S(1)} %copy-done, bf16[32,512]{1,0:T(8,128)(2,1)S(1)} %copy-done.3, bf16[32,512]{1,0:T(8,128)(2,1)S(1)} %copy-done.4, bf16[32,512]{1,0:T(8,128)(2,1)S(1)} %copy-done.5, ...), custom_call_target="tpu_custom_call" | custom-call | tf_op jit(solution)/shard_map/layer/pallas_call | solution.py:397
  73.4 0.6 copy.20
  74.0 0.9 %copy.21 = f32[3,4,128,128]{3,2,1,0:T(8,128)} copy(f32[3,4,128,128]{3,2,1,0:T(8,128)S(1)} %get-tuple-element.9) | data formatting | bytes 1572864
  (2 shorter events, 0.0 us)
Async XLA Ops:
  0.6 0.7 copy-start.12
  0.6 0.7 copy-start.13
  0.7 0.8 %copy-start.10 = (bf16[32,4]{0,1:T(4,128)(2,1)S(1)}, bf16[32,4]{0,1:T(4,128)(2,1)}, u32[]{:S(2)}) copy-start(bf16[32,4]{0,1:T(4,128)(2,1)} %param.21) | copy-start | bytes 772
  0.7 0.8 %copy-start.11 = (bf16[32,4]{0,1:T(4,128)(2,1)S(1)}, bf16[32,4]{0,1:T(4,128)(2,1)}, u32[]{:S(2)}) copy-start(bf16[32,4]{0,1:T(4,128)(2,1)} %param.20) | copy-start | bytes 772
  0.7 0.8 %copy-start.9 = (bf16[192,16]{0,1:T(8,128)(2,1)S(1)}, bf16[192,16]{0,1:T(8,128)(2,1)}, u32[]{:S(2)}) copy-start(bf16[192,16]{0,1:T(8,128)(2,1)} %param.14) | copy-start | bytes 18436
  1.3 0.8 %copy-start.4 = (bf16[32,512]{1,0:T(8,128)(2,1)S(1)}, bf16[32,512]{1,0:T(8,128)(2,1)}, u32[]{:S(2)}) copy-start(bf16[32,512]{1,0:T(8,128)(2,1)} %wk_hbm.1) | copy-start | bytes 98308
  1.4 0.8 %copy-start.3 = (bf16[32,512]{1,0:T(8,128)(2,1)S(1)}, bf16[32,512]{1,0:T(8,128)(2,1)}, u32[]{:S(2)}) copy-start(bf16[32,512]{1,0:T(8,128)(2,1)} %wq_hbm.1) | copy-start | bytes 98308
  1.5 0.7 copy-start.7
  1.5 0.7 copy-start.8
  2.2 1.1 %copy-start = (f32[3,4,128,128]{3,2,1,0:T(8,128)S(1)}, f32[3,4,128,128]{3,2,1,0:T(8,128)}, u32[]{:S(2)}) copy-start(f32[3,4,128,128]{3,2,1,0:T(8,128)} %state_hbm.1) | copy-start | bytes 2359300
  3.3 0.9 %copy-start.1 = (bf16[2048,64]{0,1:T(8,128)(2,1)S(1)}, bf16[2048,64]{0,1:T(8,128)(2,1)}, u32[]{:S(2)}) copy-start(bf16[2048,64]{0,1:T(8,128)(2,1)} %param.26) | copy-start | bytes 786436
  4.3 0.9 %copy-start.2 = (bf16[64,2048]{1,0:T(8,128)(2,1)S(1)}, bf16[64,2048]{1,0:T(8,128)(2,1)}, u32[]{:S(2)}) copy-start(bf16[64,2048]{1,0:T(8,128)(2,1)} %wd_hbm.1) | copy-start | bytes 786436
  5.2 0.8 %copy-start.5 = (bf16[32,512]{1,0:T(8,128)(2,1)S(1)}, bf16[32,512]{1,0:T(8,128)(2,1)}, u32[]{:S(2)}) copy-start(bf16[32,512]{1,0:T(8,128)(2,1)} %wv_hbm.1) | copy-start | bytes 98308
  6.0 0.8 %copy-start.6 = (bf16[512,32]{0,1:T(8,128)(2,1)S(1)}, bf16[512,32]{0,1:T(8,128)(2,1)}, u32[]{:S(2)}) copy-start(bf16[512,32]{0,1:T(8,128)(2,1)} %param.24) | copy-start | bytes 98308

commit v2 on v1

--- a/solution.py
+++ b/solution.py
@@ -15,6 +15,7 @@
 BF16 = jnp.bfloat16
 NT = (((1,), (1,)), ((), ()))
 R1 = 40
+GATE_AT = 200
 R3 = 32
 
 
@@ -23,7 +24,13 @@
 
 
 def body(
-    tile_hbm,
+    tokens_hbm,
+    mix_gain_hbm,
+    ff_gain_hbm,
+    beta_hbm,
+    decay_hbm,
+    head_gain_hbm,
+    decay_log_hbm,
     state_hbm,
     wq_hbm,
     wk_hbm,
@@ -31,16 +38,22 @@
     wo_hbm,
     wu_hbm,
     wd_hbm,
-    head_gain_ref,
-    decay_log_ref,
     out_ref,
-    state_out,
+    vec_ref,
+    tok,
+    mixg,
+    ffg,
+    bta,
+    dcy,
+    hgain,
+    dlog,
     tbuf,
     wbuf,
     wo,
     fbuf,
     st,
     qbuf,
+    ebuf,
     xs,
     zs,
     zsend,
@@ -61,6 +74,10 @@
     lsem,
     ssem,
     rsem,
+    fsem,
+    near_sem,
+    mid_sem,
+    far_sem,
 ):
     kv = lax.axis_index("kv")
     tp = lax.axis_index("tp")
@@ -71,41 +88,42 @@
 
     barrier = pltpu.get_barrier_semaphore()
 
-    def greet_z(j, carry):
-        t = (z * 2 + tp + j) % (2 * NZ)
-        pl.semaphore_signal(
-            barrier, inc=1, device_id={"kv": (t // 2) * NY + y, "tp": t % 2}, device_id_type=MESH
-        )
+    def greet(sem, where):
+        pl.semaphore_signal(sem, inc=1, device_id=where, device_id_type=MESH)
+
+    def on_ring(d):
+        return {"kv": ((z + d) % NZ) * NY + y}
+
+    def greet_eight(j, carry):
+        p = (me8 + j) % 8
+        greet(barrier, {"kv": z * NY + p // 2, "tp": p % 2})
         return carry
 
-    lax.fori_loop(1, 2 * NZ, greet_z, 0)
-
-    def greet_y(j, carry):
-        other = z * NY + (y + j) % NY
-        for t in range(2):
-            pl.semaphore_signal(
-                barrier, inc=1, device_id={"kv": other, "tp": t}, device_id_type=MESH
-            )
-        return carry
-
-    lax.fori_loop(1, NY, greet_y, 0)
+    lax.fori_loop(1, 8, greet_eight, 0)
+    greet(barrier, on_ring(1))
+    greet(barrier, on_ring(NZ - 1))
 
     def local(src, dst, k):
         return pltpu.make_async_copy(src, dst, lsem.at[k])
 
+    my_wo = wo.at[
+        pl.ds(pl.multiple_of(y * 32, 32), 32), pl.ds(pl.multiple_of(tp * 512, 512), 512)
+    ]
     loads = [
-        local(tile_hbm, tbuf.at[me8], 0),
-        local(wq_hbm, wbuf.at[y, 0], 1),
-        local(wk_hbm, wbuf.at[y, 1], 2),
-        local(wv_hbm, wbuf.at[y, 2], 3),
-        local(
-            wo_hbm,
-            wo.at[pl.ds(pl.multiple_of(y * 32, 32), 32), pl.ds(pl.multiple_of(tp * 512, 512), 512)],
-            4,
-        ),
-        local(wu_hbm, fbuf.at[tp, y, 0], 5),
-        local(wd_hbm, fbuf.at[tp, y, 1], 6),
-        local(state_hbm, st, 7),
+        local(tokens_hbm, tok, 0),
+        local(mix_gain_hbm, mixg, 1),
+        local(ff_gain_hbm, ffg, 2),
+        local(beta_hbm, bta, 3),
+        local(decay_hbm, dcy, 4),
+        local(wq_hbm, wbuf.at[y, 0], 5),
+        local(wk_hbm, wbuf.at[y, 1], 6),
+        local(wv_hbm, wbuf.at[y, 2], 7),
+        local(wo_hbm, my_wo, 8),
+        local(wu_hbm, fbuf.at[tp, y, 0], 9),
+        local(wd_hbm, fbuf.at[tp, y, 1], 10),
+        local(head_gain_hbm, hgain, 11),
+        local(decay_log_hbm, dlog, 12),
+        local(state_hbm, st, 13),
     ]
     for c in loads:
         c.start()
@@ -119,20 +137,38 @@
     wanted = jnp.where(row < 48, 12 * (row % 16) + 3 * y + row // 16, row + 144)
     pick = jnp.where((col == wanted) & (row < 50), 1.0, 0.0).astype(BF16)
 
-    er, ec = iota((512, 128), 0), iota((512, 128), 1)
-    spread = jnp.where((ec == er // 128 * 32 + er % 128) & (er % 128 < 32), 1.0, 0.0).astype(BF16)
-
-    for c in loads[:7]:
+    er, ec = iota((1024, 128), 0), iota((1024, 128), 1)
+    into = er % 256 - GATE_AT
+    spread = jnp.where((ec == er // 256 * 32 + into) & (into >= 0) & (into < 32), 1.0, 0.0)
+    ebuf[...] = spread.astype(BF16)
+    pr, pc = iota((32, 256), 0), iota((32, 256), 1)
+    shift = jnp.where(pc == pr + GATE_AT, 1.0, 0.0).astype(BF16)
+
+    for c in loads[:5]:
         c.wait()
-
-    pl.semaphore_wait(barrier, 2 * NZ - 1 + 2 * (NY - 1))
-
-    def push(src, dst, k, where):
+    sr, sc = iota((16, 16), 0), iota((16, 16), 1)
+
+    def upright(ref):
+        return jnp.sum(jnp.where(sr == sc, ref[...].astype(F32), 0.0), axis=1, keepdims=True)
+
+    gate_rows = jnp.concatenate([bta[...].astype(F32), dcy[...].astype(F32)], axis=0)
+    gate_rows = jnp.concatenate([gate_rows, jnp.zeros((8, 32), F32)], axis=0).astype(BF16)
+    lanes = iota((16, 256), 1)
+    tile = jnp.dot(gate_rows, shift, preferred_element_type=F32)
+    tile = jnp.where(lanes == 192, upright(mixg), jnp.where(lanes == 193, upright(ffg), tile))
+    tile = tile + jnp.concatenate([tok[...].astype(F32), jnp.zeros((16, 64), F32)], axis=1)
+    tbuf[me8] = tile.astype(BF16)
+    for c in loads[5:11]:
+        c.wait()
+
+    pl.semaphore_wait(barrier, 9)
+
+    def push(src, dst, k, where, to=None):
         pltpu.make_async_remote_copy(
             src_ref=src,
             dst_ref=dst,
             send_sem=ssem.at[k],
-            recv_sem=rsem.at[k],
+            recv_sem=rsem.at[k] if to is None else to,
             device_id=where,
             device_id_type=MESH,
         ).start()
@@ -145,41 +181,56 @@
 
         lax.fori_loop(1, 8, one, 0)
 
-    def to_column(ref, k):
-        def one(j, carry):
-            push(ref, ref, k, {"kv": z * NY + (y + j) % NY})
-            return carry
-
-        lax.fori_loop(1, NY, one, 0)
+    above, below, across = (y + 1) % NY, (y + NY - 1) % NY, (y + 2) % NY
+
+    def at_y(other):
+        return {"kv": z * NY + other}
 
     def got(ref, sem):
         pltpu.make_async_copy(ref, ref, sem).wait()
 
-    my_wo = wo.at[
-        pl.ds(pl.multiple_of(y * 32, 32), 32), pl.ds(pl.multiple_of(tp * 512, 512), 512)
-    ]
     to_eight(lambda p: tbuf.at[me8], tbuf.at[me8], 0)
-    to_column(wbuf.at[y], 1)
-    to_eight(lambda p: my_wo, my_wo, 2)
-    to_column(fbuf.at[tp, y], 3)
+    push(wbuf.at[y], wbuf.at[y], 1, at_y(above), fsem.at[0])
+    push(wbuf.at[y], wbuf.at[y], 1, at_y(below), fsem.at[1])
+    greet(near_sem, on_ring(1))
+    greet(near_sem, on_ring(NZ - 1))
+    pl.semaphore_wait(near_sem, 2)
+    greet(mid_sem, on_ring(2))
+    greet(mid_sem, on_ring(NZ - 2))
+    pl.semaphore_wait(mid_sem, 2)
+    greet(far_sem, on_ring(4))
+    greet(far_sem, on_ring(NZ - 4))
+    got(wbuf.at[y], fsem.at[0])
+    upper_half = wbuf.at[below, :, pl.ds(0, 16)]
+    push(upper_half, upper_half, 2, at_y(above), fsem.at[2])
+    got(wbuf.at[y], fsem.at[1])
+    lower_half = wbuf.at[above, :, pl.ds(16, 16)]
+    push(lower_half, lower_half, 2, at_y(below), fsem.at[3])
+    for other in (above, below, across):
+        push(my_wo, my_wo, 10, at_y(other))
+    push(fbuf.at[tp, y], fbuf.at[tp, y], 3, at_y(above), fsem.at[4])
+    push(fbuf.at[tp, y], fbuf.at[tp, y], 3, at_y(below), fsem.at[5])
+    push(fbuf.at[tp, y], fbuf.at[tp, y], 7, {"tp": 1 - tp}, fsem.at[8])
 
     got(tbuf.at[pl.ds(0, 7)], rsem.at[0])
     tiles = tbuf[...]
-    turned = tiles[:, :16, :].reshape(128, 256)
+    turned = tiles.reshape(128, 256)
     chosen = lax.dot_general(pick, turned, NT, preferred_element_type=F32)
     xs[...] = chosen
     x = chosen[:48]
     scaled = (x * chosen[48:49]).astype(BF16)
     square = jnp.sum(x * x, axis=1, keepdims=True)
     square_hi = square.astype(BF16).astype(F32)
-    own = jnp.concatenate([tbuf[2 * k + tp, 16:32, :128] for k in range(NY)], axis=1)
-    gate_w = jnp.dot(own, spread, preferred_element_type=F32).astype(BF16)
+    own = jnp.concatenate([tbuf[2 * k + tp] for k in range(NY)], axis=1)
+    gate_w = jnp.dot(own, ebuf[...], preferred_element_type=F32)
+    gate_w = jnp.where(iota((16, 128), 0) < 8, gate_w, 0.0).astype(BF16)
     gate_w = jnp.concatenate([gate_w, jnp.zeros((112, 128), BF16)], axis=0)
     gate = lax.dot_general(scaled, gate_w, NT, preferred_element_type=F32)
     gl = iota((48, 128), 1)
     gate = jnp.where(gl == 8, square_hi, jnp.where(gl == 9, square - square_hi, gate))
 
-    got(wbuf.at[pl.ds(0, 3)], rsem.at[1])
+    got(upper_half, fsem.at[2])
+    got(lower_half, fsem.at[3])
     for m in range(3):
         weight = wbuf[:, m].reshape(128, 512)
         part = jnp.dot(scaled, weight, preferred_element_type=F32)
@@ -193,6 +244,8 @@
     zs[pl.ds(39, NZ, R1), :] = jnp.zeros((NZ, 128), F32)
     zsend[...] = zs[...].reshape(NZ, R1, 128).astype(BF16)
 
+    pl.semaphore_wait(far_sem, 2)
+
     def along(src_of, dst, k):
         def one(n, carry):
             d = NZ // 2 + ((n + 1) // 2) * (1 - 2 * (n % 2))
@@ -204,7 +257,8 @@
 
     along(lambda far: zsend.at[far], zrecv.at[z], 4)
     zrecv[z] = zsend[z]
-    loads[7].wait()
+    for c in loads[11:]:
+        c.wait()
     got(zrecv.at[pl.ds(0, NZ - 1)], rsem.at[4])
 
     acc = zrecv[0].astype(F32)
@@ -224,12 +278,8 @@
     beta = jax.nn.sigmoid(inverse * take(l12 == head_of))
     u = inverse * take(l12 == head_of + 4)
     soft = jnp.maximum(u, 0.0) + jnp.log1p(jnp.exp(-jnp.abs(u)))
-    h1 = iota((12, 1), 0) // 3
-    rate = jnp.where(
-        h1 == 0,
-        decay_log_ref[0],
-        jnp.where(h1 == 1, decay_log_ref[1], jnp.where(h1 == 2, decay_log_ref[2], decay_log_ref[3])),
-    )
+    lr, lc = iota((12, 4), 0), iota((12, 4), 1)
+    rate = jnp.sum(jnp.where(lc == lr // 3, dlog[...], 0.0), axis=1, keepdims=True)
     keep = jnp.exp(-jnp.exp(rate) * soft)
     query = inverse * accs[0:12, :]
     key = inverse * accs[12:24, :]
@@ -246,19 +296,19 @@
         qc = both[:, r : r + 1]
         kept = st[i, h] * keep[r : r + 1, :]
         predicted = jnp.sum(kept * kc, axis=0, keepdims=True)
-        new = kept + kc * (beta[r : r + 1, :] * (value[r : r + 1, :] - predicted))
-        st[i, h] = new
-        hs[r : r + 1, :] = jnp.sum(new * qc, axis=0, keepdims=True)
+        change = beta[r : r + 1, :] * (value[r : r + 1, :] - predicted)
+        vec_ref[12 + r : 13 + r, :] = change
+        hs[r : r + 1, :] = jnp.sum((kept + kc * change) * qc, axis=0, keepdims=True)
+    vec_ref[0:12, :] = knorm
+    vec_ref[24:36, :] = jnp.broadcast_to(keep, (12, 128))
     heads = hs[...] / jnp.sqrt(jnp.float32(128))
     heads = jnp.where(iota((16, 128), 0) < 12, heads, 0.0)
     normed = (
         heads
         * lax.rsqrt(jnp.mean(heads * heads, axis=1, keepdims=True) + 1e-06)
-        * head_gain_ref[...].astype(F32)
+        * hgain[...].astype(F32)
     )
     nsend[...] = normed.astype(BF16)
-    state_copy = local(st, state_out, 8)
-    state_copy.start()
 
     slot = (z % 8) * 2 + tp
 
@@ -273,14 +323,32 @@
     @pl.when(half == tp)
     def _():
         nrecv[slot] = nsend[...]
-        got(nrecv.at[pl.ds(0, 15)], rsem.at[5])
 
     @pl.when(half != tp)
     def _():
         push(nsend, nrecv.at[slot], 5, {"tp": half})
+
+    my_lanes = wo.at[:, pl.ds(pl.multiple_of(tp * 512, 512), 512)]
+    got(wo.at[pl.ds(0, 96), pl.ds(0, 512)], rsem.at[10])
+    push(my_lanes, my_lanes, 11, {"tp": 1 - tp})
+    got(fbuf.at[tp, y], fsem.at[4])
+    first = fbuf.at[tp, below, 0]
+    push(first, first, 12, at_y(above), fsem.at[6])
+    got(fbuf.at[tp, y], fsem.at[5])
+    second = fbuf.at[tp, above, 1]
+    push(second, second, 12, at_y(below), fsem.at[7])
+    push(fbuf.at[tp, below], fbuf.at[tp, below], 7, {"tp": 1 - tp}, fsem.at[8])
+    push(fbuf.at[tp, above], fbuf.at[tp, above], 7, {"tp": 1 - tp}, fsem.at[8])
+
+    @pl.when(half == tp)
+    def _():
+        got(nrecv.at[pl.ds(0, 15)], rsem.at[5])
+
+    @pl.when(half != tp)
+    def _():
         got(nrecv, rsem.at[5])
 
-    got(wo.at[pl.ds(0, 112), :], rsem.at[2])
+    got(my_lanes, rsem.at[11])
     nf[...] = nrecv[...].astype(F32).reshape(256, 128)
     wide = jnp.concatenate(
         [
@@ -312,8 +380,9 @@
     rsend[...] = jnp.concatenate([scaled2, tail], axis=0).astype(BF16)
     along(lambda far: rsend, rrecv.at[z], 6)
     rrecv[z] = rsend[...]
-    got(fbuf.at[tp, pl.ds(0, 3)], rsem.at[3])
-    push(fbuf.at[tp], fbuf.at[tp], 7, {"tp": 1 - tp})
+    got(first, fsem.at[6])
+    got(second, fsem.at[7])
+    push(fbuf.at[tp, across], fbuf.at[tp, across], 7, {"tp": 1 - tp}, fsem.at[8])
     got(rrecv.at[pl.ds(0, NZ - 1)], rsem.at[6])
     rows = jnp.concatenate([rrecv[k] for k in range(NZ)], axis=1)
     sums = rrecv[0, 16:32, :].astype(F32)
@@ -323,7 +392,7 @@
     scale = lax.rsqrt(squares / D + 1e-06)
     dr, dc = iota((R3, 128), 0), iota((R3, 128), 1)
     scale = jnp.sum(jnp.where(dr == dc, scale, 0.0), axis=1, keepdims=True)
-    got(fbuf.at[0], rsem.at[7])
+    got(fbuf.at[0], fsem.at[8])
     up_w = fbuf[:, :, 0].reshape(512, D)
     up = lax.dot_general(rows, up_w, NT, preferred_element_type=F32) * scale
     act = jnp.square(jnp.maximum(up, 0.0)).astype(BF16)
@@ -350,11 +419,13 @@
     placed = jnp.dot(pieces, qbuf[...], preferred_element_type=F32)
     out_ref[...] = placed[:, :192].astype(BF16)
 
-    state_copy.wait()
     got(tbuf.at[pl.ds(0, 7)], ssem.at[0])
-    got(wbuf.at[pl.ds(0, 3)], ssem.at[1])
-    got(wo.at[pl.ds(0, 112), :], ssem.at[2])
-    got(fbuf.at[tp, pl.ds(0, 3)], ssem.at[3])
+    got(wbuf.at[pl.ds(0, 2)], ssem.at[1])
+    got(wbuf.at[0], ssem.at[2])
+    got(wo.at[pl.ds(0, 96), pl.ds(0, 512)], ssem.at[10])
+    got(wo.at[:, pl.ds(0, 512)], ssem.at[11])
+    got(fbuf.at[tp, pl.ds(0, 2)], ssem.at[3])
+    got(fbuf.at[tp, y], ssem.at[12])
     got(zsend.at[pl.ds(0, NZ - 1)], ssem.at[4])
 
     @pl.when(half == tp)
@@ -369,6 +440,28 @@
     got(fbuf.at[tp], ssem.at[7])
     got(dsend.at[pl.ds(0, NZ - 1)], ssem.at[8])
     got(ysend.at[pl.ds(0, 7)], ssem.at[9])
+
+
+def finish(vec_ref, early_ref, state_hbm, out_ref, state_out, st, vt, load_sem, store_sem):
+    loads = [
+        pltpu.make_async_copy(state_hbm.at[i], st.at[i], load_sem.at[i]) for i in range(3)
+    ]
+    stores = [
+        pltpu.make_async_copy(st.at[i], state_out.at[i], store_sem.at[i]) for i in range(3)
+    ]
+    for c in loads:
+        c.start()
+    out_ref[...] = early_ref[...]
+    vt[...] = jnp.concatenate([vec_ref[0:16, :], jnp.zeros((112, 128), F32)], axis=0).T
+    for i in range(3):
+        loads[i].wait()
+        for h in range(4):
+            r = h * 3 + i
+            kept = st[i, h] * vec_ref[24 + r : 25 + r, :]
+            st[i, h] = kept + vt[:, r : r + 1] * vec_ref[12 + r : 13 + r, :]
+        stores[i].start()
+    for c in stores:
+        c.wait()
 
 
 def local_step(
@@ -387,29 +480,32 @@
     w_up,
     w_down,
 ):
-    upper = jnp.concatenate(
-        [tokens.T, mix_gain[:, None], ff_gain[:, None], jnp.zeros((16, 62), BF16)], axis=1
-    )
-    lower = jnp.concatenate([w_beta.T, w_decay.T], axis=0)
-    tile = jnp.concatenate([upper, jnp.pad(lower, ((0, 8), (0, 224)))], axis=0)
     anywhere = pl.BlockSpec(memory_space=pltpu.HBM)
     vmem = pl.BlockSpec(memory_space=pltpu.VMEM)
-    out, new_state = pl.pallas_call(
+    early, vec = pl.pallas_call(
         body,
         name="layer",
         out_shape=(
             jax.ShapeDtypeStruct((16, 192), BF16),
-            jax.ShapeDtypeStruct(state.shape, F32),
+            jax.ShapeDtypeStruct((40, 128), F32),
         ),
-        in_specs=[anywhere] * 8 + [vmem, pl.BlockSpec(memory_space=pltpu.SMEM)],
-        out_specs=(vmem, anywhere),
+        in_specs=[anywhere] * 14,
+        out_specs=(vmem, vmem),
         scratch_shapes=[
-            pltpu.VMEM((8, 32, 256), BF16),
+            pltpu.VMEM((16, 192), BF16),
+            pltpu.VMEM((1, 16), BF16),
+            pltpu.VMEM((1, 16), BF16),
+            pltpu.VMEM((4, 32), BF16),
+            pltpu.VMEM((4, 32), BF16),
+            pltpu.VMEM((1, 128), BF16),
+            pltpu.VMEM((1, 4), F32),
+            pltpu.VMEM((8, 16, 256), BF16),
             pltpu.VMEM((NY, 3, 32, 512), BF16),
             pltpu.VMEM((128, 1024), BF16),
             pltpu.VMEM((2, NY, 2, 64, D), BF16),
             pltpu.VMEM((3, 4, 128, 128), F32),
             pltpu.VMEM((1024, 256), BF16),
+            pltpu.VMEM((1024, 128), BF16),
             pltpu.VMEM((56, 128), F32),
             pltpu.VMEM((NZ * R1, 128), F32),
             pltpu.VMEM((NZ, R1, 128), BF16),
@@ -427,15 +523,25 @@
             pltpu.VMEM((NZ, 24, 128), BF16),
             pltpu.VMEM((8, 16, 128), BF16),
             pltpu.VMEM((8, 16, 128), BF16),
+            pltpu.SemaphoreType.DMA((14,)),
+            pltpu.SemaphoreType.DMA((13,)),
+            pltpu.SemaphoreType.DMA((13,)),
             pltpu.SemaphoreType.DMA((9,)),
-            pltpu.SemaphoreType.DMA((10,)),
-            pltpu.SemaphoreType.DMA((10,)),
+            pltpu.SemaphoreType.REGULAR,
+            pltpu.SemaphoreType.REGULAR,
+            pltpu.SemaphoreType.REGULAR,
         ],
         compiler_params=pltpu.CompilerParams(
-            collective_id=0, has_side_effects=True, vmem_limit_bytes=32 * 1024 * 1024
+            collective_id=0, has_side_effects=True, vmem_limit_bytes=67043328
         ),
     )(
-        tile,
+        tokens.T,
+        mix_gain[None, :],
+        ff_gain[None, :],
+        w_beta.T,
+        w_decay.T,
+        head_gain[None, :],
+        decay_log[None, :],
         state,
         w_query,
         w_key,
@@ -443,9 +549,24 @@
         w_out.T,
         w_up.T,
         w_down,
-        head_gain[None, :],
-        decay_log,
     )
+    out, new_state = pl.pallas_call(
+        finish,
+        name="finish",
+        out_shape=(
+            jax.ShapeDtypeStruct((16, 192), BF16),
+            jax.ShapeDtypeStruct(state.shape, F32),
+        ),
+        in_specs=[vmem, vmem, anywhere],
+        out_specs=(vmem, anywhere),
+        scratch_shapes=[
+            pltpu.VMEM((3, 4, 128, 128), F32),
+            pltpu.VMEM((128, 128), F32),
+            pltpu.SemaphoreType.DMA((3,)),
+            pltpu.SemaphoreType.DMA((3,)),
+        ],
+        compiler_params=pltpu.CompilerParams(vmem_limit_bytes=67043328),
+    )(vec, early, state)
     return out.T, new_state
 
 

time: 75.3 us -> 66.8 us (0.89)
  local copies, waits for them, and re-layouts: 7.43 us -> 0 us
    unnamed x30 -> x0, local copies, waits for them, and re-layouts: 7.24 us -> none
    pallas_call x1, Pallas kernels: 66.6 us -> 62.5 us  [local_step(): pl.pallas_call(body, name='layer', out_shape=(jax.ShapeDtypeStruct((16, 1...]
    pallas_call x0 -> x1, Pallas kernels: none -> 3.46 us  [local_step(): pl.pallas_call(finish, name='finish', out_shape=(jax.ShapeDtypeStruct((16...]
where the time goes in v2:
time: 66.8 us; the launch traced here: 66.6 us
  Pallas kernels  66 us (99%)
    pallas_call x1, Pallas kernels, local_step(): pl.pallas_call(body, name='layer', out_shape=(jax.ShapeDtypeStruct((16, 1...  62.5 us
    pallas_call x1, Pallas kernels, local_step(): pl.pallas_call(finish, name='finish', out_shape=(jax.ShapeDtypeStruct((16...  3.46 us

profile of v2, /device:TPU:1, one launch (start us, length us, event | category | flops | bytes accessed | tf_op | source)
XLA Modules:
  0.0 66.6 jit_solution(8302322938244153526)
XLA Ops:
  0.6 62.5 %layer.1 = (bf16[16,192]{1,0:T(8,128)(2,1)}, f32[40,128]{1,0:T(8,128)}) custom-call(bf16[16,192]{1,0:T(8,128)(2,1)} %bitcast.12, bf16[1,16]{1,0:T(2,128)(2,1)} %bitcast.15, bf16[1,16]{1,0:T(2,128)(2,1)} %bitcast.16, bf16[4,32]{1,0:T(4,128)(2,1)} %bitcast.13, bf16[4,32]{1,0:T(4,128)(2,1)} %bitcast.14, bf16[1,128]{1,0:T(2,128)(2,1)} %bitcast.17, ...), custom_call_target="tpu_custom_call" | custom-call | tf_op jit(solution)/shard_map/layer/pallas_call | solution.py:485
  63.2 3.5 %finish.1 = (bf16[16,192]{1,0:T(8,128)(2,1)}, f32[3,4,128,128]{3,2,1,0:T(8,128)}) custom-call(f32[40,128]{1,0:T(8,128)} %get-tuple-element.6.vec_ref, bf16[16,192]{1,0:T(8,128)(2,1)} %get-tuple-element.7.early_ref, f32[3,4,128,128]{3,2,1,0:T(8,128)} %state_hbm.3), custom_call_target="tpu_custom_call" | custom-call | tf_op jit(solution)/shard_map/finish/pallas_call | solution.py:553

commit v3 on v2

v3 whole, which is shorter than its diff:
```python
import functools

import jax
import jax.numpy as jnp
from jax import lax
from jax.experimental import pallas as pl
from jax.experimental.pallas import tpu as pltpu
from jax.sharding import PartitionSpec as P

D = 2048
NZ = 16
NY = 4
MESH = pl.DeviceIdType.MESH
F32 = jnp.float32
BF16 = jnp.bfloat16
NT = (((1,), (1,)), ((), ()))
R1 = 40
GATE_AT = 200


def iota(shape, dim):
    return lax.broadcasted_iota(jnp.int32, shape, dim)


def body(
    tokens_hbm,
    mix_gain_hbm,
    ff_gain_hbm,
    beta_hbm,
    decay_hbm,
    head_gain_hbm,
    decay_log_hbm,
    state_hbm,
    wq_hbm,
    wk_hbm,
    wv_hbm,
    wo_hbm,
    wu_hbm,
    wd_hbm,
    out_ref,
    vec_ref,
    tok,
    mixg,
    ffg,
    bta,
    dcy,
    hgain,
    dlog,
    tbuf,
    wbuf,
    wo,
    fbuf,
    st,
    qbuf,
    ebuf,
    xs,
    zs,
    zsend,
    zrecv,
    accs,
    g12,
    hs,
    nsend,
    nrecv,
    nf,
    xrecv,
    rrecv,
    srecv,
    xw,
    res,
    dsend,
    drecv,
    ysend,
    yrecv,
    lsem,
    ssem,
    rsem,
    fsem,
    near_sem,
    mid_sem,
    far_sem,
):
    kv = lax.axis_index("kv")
    tp = lax.axis_index("tp")
    z = kv // NY
    y = kv % NY
    me8 = y * 2 + tp
    half = z // 8

    barrier = pltpu.get_barrier_semaphore()

    def local(src, dst, k):
        return pltpu.make_async_copy(src, dst, lsem.at[k])

    def mine(block):
        return wo.at[
            block,
            pl.ds(pl.multiple_of(y * 32, 32), 32),
            pl.ds(pl.multiple_of(tp * 512, 512), 512),
        ]

    loads = [
        local(wq_hbm, wbuf.at[y, 0], 5),
        local(wk_hbm, wbuf.at[y, 1], 6),
        local(wv_hbm, wbuf.at[y, 2], 7),
        local(tokens_hbm, tok, 0),
        local(mix_gain_hbm, mixg, 1),
        local(ff_gain_hbm, ffg, 2),
        local(beta_hbm, bta, 3),
        local(decay_hbm, dcy, 4),
        local(wo_hbm, mine(0), 8),
        local(wu_hbm, fbuf.at[tp, y, 0], 9),
        local(wd_hbm, fbuf.at[tp, y, 1], 10),
        local(head_gain_hbm, hgain, 11),
        local(decay_log_hbm, dlog, 12),
        local(state_hbm, st, 13),
    ]
    for c in loads:
        c.start()

    def greet(sem, where):
        pl.semaphore_signal(sem, inc=1, device_id=where, device_id_type=MESH)

    def on_ring(d):
        return {"kv": ((z + d) % NZ) * NY + y}

    def greet_eight(j, carry):
        p = (me8 + j) % 8
        greet(barrier, {"kv": z * NY + p // 2, "tp": p % 2})
        return carry

    lax.fori_loop(1, 8, greet_eight, 0)
    greet(barrier, on_ring(1))
    greet(barrier, on_ring(NZ - 1))

    for c in loads[:3]:
        c.wait()

    pl.semaphore_wait(barrier, 9)

    def push(src, dst, k, where, to=None):
        pltpu.make_async_remote_copy(
            src_ref=src,
            dst_ref=dst,
            send_sem=ssem.at[k],
            recv_sem=rsem.at[k] if to is None else to,
            device_id=where,
            device_id_type=MESH,
        ).start()

    def to_eight(src_of, dst, k):
        def one(j, carry):
            p = (me8 + j) % 8
            push(src_of(p), dst, k, {"kv": z * NY + p // 2, "tp": p % 2})
            return carry

        lax.fori_loop(1, 8, one, 0)

    above, below, across = (y + 1) % NY, (y + NY - 1) % NY, (y + 2) % NY

    sibling = {"tp": 1 - tp}

    def at_y(other):
        return {"kv": z * NY + other}

    def got(ref, sem):
        pltpu.make_async_copy(ref, ref, sem).wait()

    high, low = pl.ds(0, 16), pl.ds(16, 16)
    for part, k in ((high, 0), (low, 1)):
        push(wbuf.at[y, :, part], wbuf.at[y, :, part], 1, at_y(above), fsem.at[k])
    for part, k in ((low, 2), (high, 3)):
        push(wbuf.at[y, :, part], wbuf.at[y, :, part], 1, at_y(below), fsem.at[k])
    greet(near_sem, on_ring(1))
    greet(near_sem, on_ring(NZ - 1))

    row, col = iota((56, 256), 0), iota((56, 256), 1)
    wanted = jnp.where(row < 48, 12 * (row % 16) + 3 * y + row // 16, row + 144)
    pick = jnp.where((col == wanted) & (row < 50), 1.0, 0.0).astype(BF16)

    pr, pc = iota((32, 256), 0), iota((32, 256), 1)
    shift = jnp.where(pc == pr + GATE_AT, 1.0, 0.0).astype(BF16)

    for c in loads[3:8]:
        c.wait()
    sr, sc = iota((16, 16), 0), iota((16, 16), 1)

    def upright(ref):
        return jnp.sum(jnp.where(sr == sc, ref[...].astype(F32), 0.0), axis=1, keepdims=True)

    gate_rows = jnp.concatenate([bta[...].astype(F32), dcy[...].astype(F32)], axis=0)
    gate_rows = jnp.concatenate([gate_rows, jnp.zeros((8, 32), F32)], axis=0).astype(BF16)
    lanes = iota((16, 256), 1)
    tile = jnp.dot(gate_rows, shift, preferred_element_type=F32)
    tile = jnp.where(lanes == 192, upright(mixg), jnp.where(lanes == 193, upright(ffg), tile))
    tile = tile + jnp.concatenate([tok[...].astype(F32), jnp.zeros((16, 64), F32)], axis=1)
    tbuf[me8] = tile.astype(BF16)
    to_eight(lambda p: tbuf.at[me8], tbuf.at[me8], 0)
    pl.semaphore_wait(near_sem, 2)
    greet(mid_sem, on_ring(2))
    greet(mid_sem, on_ring(NZ - 2))
    er, ec = iota((1024, 128), 0), iota((1024, 128), 1)
    into = er % 256 - GATE_AT
    spread = jnp.where((ec == er // 256 * 32 + into) & (into >= 0) & (into < 32), 1.0, 0.0)
    ebuf[...] = spread.astype(BF16)
    pl.semaphore_wait(mid_sem, 2)
    greet(far_sem, on_ring(4))
    greet(far_sem, on_ring(NZ - 4))
    for c in loads[8:11]:
        c.wait()
    push(mine(0), mine(3), 10, on_ring(4))
    push(mine(0), mine(1), 10, on_ring(NZ - 4))
    got(wbuf.at[y, :, high], fsem.at[0])
    push(wbuf.at[below, :, high], wbuf.at[below, :, high], 2, at_y(above), fsem.at[4])
    got(wbuf.at[y, :, low], fsem.at[2])
    push(wbuf.at[above, :, low], wbuf.at[above, :, low], 2, at_y(below), fsem.at[5])
    for other, k in ((above, 6), (below, 7)):
        push(fbuf.at[tp, y, 0], fbuf.at[tp, y, 0], 3, at_y(other), fsem.at[k])
    push(fbuf.at[tp, y], fbuf.at[tp, y], 7, sibling, fsem.at[12])
    pl.semaphore_wait(far_sem, 2)
    push(mine(0), mine(2), 10, on_ring(8))
    got(tbuf.at[pl.ds(0, 7)], rsem.at[0])
    tiles = tbuf[...]
    turned = tiles.reshape(128, 256)
    chosen = lax.dot_general(pick, turned, NT, preferred_element_type=F32)
    xs[...] = chosen
    gain_rows = jnp.where(iota((8, 128), 0) == 0, chosen[49:50], 0.0)
    token_rows = [xs[pl.ds(pl.multiple_of(i * 16 + tp * 8, 8), 8), :] for i in range(3)]
    xrecv[0] = jnp.concatenate(token_rows + [gain_rows], axis=0).astype(BF16)
    push(xrecv.at[0], xrecv.at[3], 8, on_ring(4))
    push(xrecv.at[0], xrecv.at[1], 8, on_ring(NZ - 4))
    push(xrecv.at[0], xrecv.at[2], 8, on_ring(8))
    x = chosen[:48]
    scaled = (x * chosen[48:49]).astype(BF16)
    square = jnp.sum(x * x, axis=1, keepdims=True)
    square_hi = square.astype(BF16).astype(F32)
    own = jnp.concatenate([tbuf[2 * k + tp] for k in range(NY)], axis=1)
    gate_w = jnp.dot(own, ebuf[...], preferred_element_type=F32)
    gate_w = jnp.where(iota((16, 128), 0) < 8, gate_w, 0.0).astype(BF16)
    gate_w = jnp.concatenate([gate_w, jnp.zeros((112, 128), BF16)], axis=0)
    gate = lax.dot_general(scaled, gate_w, NT, preferred_element_type=F32)
    gl = iota((48, 128), 1)
    gate = jnp.where(gl == 8, square_hi, jnp.where(gl == 9, square - square_hi, gate))

    got(wbuf.at[y, :, low], fsem.at[1])
    got(wbuf.at[y, :, high], fsem.at[3])
    got(wbuf.at[y, :, high], fsem.at[4])
    got(wbuf.at[y, :, low], fsem.at[5])
    for m in range(3):
        weight = wbuf[:, m].reshape(128, 512)
        part = jnp.dot(scaled, weight, preferred_element_type=F32)
        for h in range(4):
            for i in range(3):
                zs[pl.ds(m * 12 + h * 3 + i, NZ, R1), :] = part[
                    i * 16 : (i + 1) * 16, h * 128 : (h + 1) * 128
                ]
    for i in range(3):
        zs[pl.ds(36 + i, NZ, R1), :] = gate[i * 16 : (i + 1) * 16]
    zs[pl.ds(39, NZ, R1), :] = jnp.zeros((NZ, 128), F32)
    zsend[...] = zs[...].reshape(NZ, R1, 128).astype(BF16)

    def along(src_of, dst, k):
        def one(n, carry):
            d = NZ // 2 + ((n + 1) // 2) * (1 - 2 * (n % 2))
            far = (z + d) % NZ
            push(src_of(far), dst, k, {"kv": far * NY + y})
            return carry

        lax.fori_loop(0, NZ - 1, one, 0)

    along(lambda far: zsend.at[far], zrecv.at[z], 4)
    zrecv[z] = zsend[z]
    for c in loads[11:]:
        c.wait()
    src_row, seq_col = iota((1024, 256), 0), iota((1024, 256), 1)
    lane = src_row % 128
    place = 12 * ((src_row // 128 % 2) * 8 + lane % 8) + 3 * (src_row // 256) + lane // 8
    qbuf[...] = jnp.where((seq_col == place) & (lane < 24), 1.0, 0.0).astype(BF16)

    def column(other, blocks):
        return wo.at[
            blocks,
            pl.ds(pl.multiple_of(other * 32, 32), 32),
            pl.ds(pl.multiple_of(tp * 512, 512), 512),
        ]

    every, first, last = pl.ds(0, 4), pl.ds(0, 2), pl.ds(2, 2)
    got(column(y, pl.ds(0, 3)), rsem.at[10])
    for other, k in ((above, 8), (below, 9)):
        push(column(y, every), column(y, every), 11, at_y(other), fsem.at[k])
    for other, k in ((above, 10), (below, 11)):
        push(fbuf.at[tp, y, 1], fbuf.at[tp, y, 1], 3, at_y(other), fsem.at[k])
    got(zrecv.at[pl.ds(0, NZ - 1)], rsem.at[4])

    acc = zrecv[0].astype(F32)
    for k in range(1, NZ):
        acc = acc + zrecv[k].astype(F32)
    accs[...] = acc
    for h in range(4):
        g12[3 * h : 3 * h + 3, :] = accs[36:39, :]
    g = g12[0:12, :]
    r12, l12 = iota((12, 128), 0), iota((12, 128), 1)
    head_of = r12 // 3

    def take(mask):
        return jnp.sum(jnp.where(mask, g, 0.0), axis=1, keepdims=True)

    inverse = lax.rsqrt(take((l12 == 8) | (l12 == 9)) / D + 1e-06)
    beta = jax.nn.sigmoid(inverse * take(l12 == head_of))
    u = inverse * take(l12 == head_of + 4)
    soft = jnp.maximum(u, 0.0) + jnp.log1p(jnp.exp(-jnp.abs(u)))
    lr, lc = iota((12, 4), 0), iota((12, 4), 1)
    rate = jnp.sum(jnp.where(lc == lr // 3, dlog[...], 0.0), axis=1, keepdims=True)
    keep = jnp.exp(-jnp.exp(rate) * soft)
    query = inverse * accs[0:12, :]
    key = inverse * accs[12:24, :]
    value = inverse * accs[24:36, :]
    qnorm = query * lax.rsqrt(jnp.sum(query * query, axis=1, keepdims=True) + 1e-06)
    knorm = key * lax.rsqrt(jnp.sum(key * key, axis=1, keepdims=True) + 1e-06)
    pad = jnp.zeros((104, 128), F32)
    g12[0:12, :] = qnorm
    g12[12:24, :] = knorm
    both = jnp.concatenate([g12[...], pad], axis=0).T
    for r in range(12):
        h, i = r // 3, r % 3
        kc = both[:, 12 + r : 13 + r]
        qc = both[:, r : r + 1]
        kept = st[i, h] * keep[r : r + 1, :]
        predicted = jnp.sum(kept * kc, axis=0, keepdims=True)
        change = beta[r : r + 1, :] * (value[r : r + 1, :] - predicted)
        vec_ref[12 + r : 13 + r, :] = change
        hs[r : r + 1, :] = jnp.sum((kept + kc * change) * qc, axis=0, keepdims=True)
    vec_ref[0:12, :] = knorm
    vec_ref[24:36, :] = jnp.broadcast_to(keep, (12, 128))
    heads = hs[...] / jnp.sqrt(jnp.float32(128))
    heads = jnp.where(iota((16, 128), 0) < 12, heads, 0.0)
    normed = (
        heads
        * lax.rsqrt(jnp.mean(heads * heads, axis=1, keepdims=True) + 1e-06)
        * hgain[...].astype(F32)
    )
    nsend[...] = normed.astype(BF16)

    slot = (z % 8) * 2 + tp

    def spread_heads(n, carry):
        d = (NZ // 2 + ((n + 1) // 2) * (1 - 2 * (n % 2))) % NZ
        far = (z + d) % NZ
        push(nsend, nrecv.at[slot], 5, {"kv": far * NY + y, "tp": half})
        return carry

    lax.fori_loop(0, NZ - 1, spread_heads, 0)

    @pl.when(half == tp)
    def _():
        nrecv[slot] = nsend[...]

    @pl.when(half != tp)
    def _():
        push(nsend, nrecv.at[slot], 5, {"tp": half})

    ahead, behind = pl.ds(0, 32), pl.ds(32, 32)
    got(column(y, every), fsem.at[8])
    push(column(below, first), column(below, first), 2, at_y(above), fsem.at[13])
    got(column(y, every), fsem.at[9])
    push(column(above, last), column(above, last), 2, at_y(below), fsem.at[14])
    for m, (a, b, c, d) in ((0, (6, 7, 15, 16)), (1, (10, 11, 17, 18))):
        got(fbuf.at[tp, y, m], fsem.at[a])
        push(
            fbuf.at[tp, below, m, ahead], fbuf.at[tp, below, m, ahead], 9, at_y(above), fsem.at[c]
        )
        got(fbuf.at[tp, y, m], fsem.at[b])
        push(
            fbuf.at[tp, above, m, behind],
            fbuf.at[tp, above, m, behind],
            9,
            at_y(below),
            fsem.at[d],
        )
        for other in (above, below):
            push(fbuf.at[tp, other, m], fbuf.at[tp, other, m], 7, sibling, fsem.at[12])
    got(column(y, first), fsem.at[13])
    got(column(y, last), fsem.at[14])
    my_lanes = wo.at[:, :, pl.ds(pl.multiple_of(tp * 512, 512), 512)]
    push(my_lanes, my_lanes, 12, sibling)
    @pl.when(half == tp)
    def _():
        got(nrecv.at[pl.ds(0, 15)], rsem.at[5])

    @pl.when(half != tp)
    def _():
        got(nrecv, rsem.at[5])

    got(my_lanes, rsem.at[12])
    got(xrecv.at[pl.ds(0, 3)], rsem.at[8])
    nf[...] = nrecv[...].astype(F32).reshape(256, 128)
    wide = jnp.concatenate(
        [
            jnp.concatenate(
                [nf[pl.ds(t * 16 + h * 3 + i, 8, 32), :] for i in range(3)], axis=0
            )
            for t in range(2)
            for h in range(4)
        ],
        axis=1,
    ).astype(BF16)
    spent = jnp.zeros((24, 128), F32)
    for j in range(4):
        mixed = lax.dot_general(wide, wo[j], NT, preferred_element_type=F32)
        known = xrecv[j].astype(F32)
        resid = (known[:24] + mixed).astype(BF16).astype(F32)
        if j == 0:
            res[...] = resid
        rrecv[0, j] = (resid * known[24:25]).astype(BF16)
        spent = spent + resid * resid
    total = lax.dot_general(
        jnp.ones((8, 128), F32),
        jnp.concatenate([spent, jnp.zeros((104, 128), F32)], axis=0),
        NT,
        preferred_element_type=F32,
        precision=lax.Precision.HIGHEST,
    )
    total_hi = total.astype(BF16).astype(F32)
    r8 = iota((8, 128), 0)
    tail = jnp.where(r8 == 0, total_hi, jnp.where(r8 == 1, total - total_hi, 0.0))
    srecv[0] = tail.astype(BF16)
    for slot_at, d in ((3, NZ - 2), (1, NZ - 1), (2, 1)):
        push(rrecv.at[0], rrecv.at[slot_at], 6, on_ring(d))
        push(srecv.at[0], srecv.at[slot_at], 5, on_ring(d), rsem.at[7])
    for m, (a, b) in ((0, (15, 16)), (1, (17, 18))):
        got(fbuf.at[tp, y, m, ahead], fsem.at[a])
        got(fbuf.at[tp, y, m, behind], fsem.at[b])
        push(fbuf.at[tp, across, m], fbuf.at[tp, across, m], 7, sibling, fsem.at[12])
    got(rrecv.at[pl.ds(0, 3)], rsem.at[6])
    got(srecv.at[pl.ds(0, 3)], rsem.at[7])
    for k, off in enumerate((0, 1, NZ - 1, 2)):
        for j in range(4):
            at = pl.multiple_of((z + off + 4 * j) % NZ * 128, 128)
            xw[:, pl.ds(at, 128)] = rrecv[k, j]
    sums = srecv[0].astype(F32)
    for k in range(1, 4):
        sums = sums + srecv[k].astype(F32)
    squares = sums[0:1] + sums[1:2]
    scale = lax.rsqrt(squares / D + 1e-06)
    dr, dc = iota((24, 128), 0), iota((24, 128), 1)
    scale = jnp.sum(jnp.where(dr == dc, scale, 0.0), axis=1, keepdims=True)
    got(fbuf.at[0], fsem.at[12])
    up_w = fbuf[:, :, 0].reshape(512, D)
    up = lax.dot_general(xw[...], up_w, NT, preferred_element_type=F32) * scale
    act = jnp.square(jnp.maximum(up, 0.0)).astype(BF16)
    for group in ((8, 7, 9, 6), (10, 5, 11, 4), (12, 3, 13, 2), (14, 1, 15, 0)):
        away = [(z + d) % NZ for d in group]
        down_w = jnp.concatenate(
            [
                fbuf[:, :, 1, :, pl.ds(pl.multiple_of(far * 128, 128), 128)].reshape(512, 128)
                for far in away
            ],
            axis=1,
        )
        part = jnp.dot(act, down_w, preferred_element_type=F32).astype(BF16)
        for n, (d, far) in enumerate(zip(group, away)):
            dsend[far] = part[:, n * 128 : (n + 1) * 128]
            if d:
                push(dsend.at[far], drecv.at[z], 13, {"kv": far * NY + y})
    drecv[z] = dsend[z]
    got(drecv.at[pl.ds(0, NZ - 1)], rsem.at[13])
    final = res[...]
    for k in range(NZ):
        final = final + drecv[k].astype(F32)
    final = jnp.concatenate([final, jnp.zeros((104, 128), F32)], axis=0).T
    ysend[...] = final.astype(BF16).reshape(8, 16, 128)
    to_eight(lambda p: ysend.at[p], yrecv.at[me8], 14)
    yrecv[me8] = ysend[me8]
    got(yrecv.at[pl.ds(0, 7)], rsem.at[14])
    pieces = jnp.concatenate([yrecv[k] for k in range(8)], axis=1)
    placed = jnp.dot(pieces, qbuf[...], preferred_element_type=F32)
    out_ref[...] = placed[:, :192].astype(BF16)

    got(tbuf.at[pl.ds(0, 7)], ssem.at[0])
    got(wbuf.at[pl.ds(0, 2)], ssem.at[1])
    got(wbuf.at[0], ssem.at[2])
    got(wo.at[pl.ds(0, 2), pl.ds(0, 64), pl.ds(0, 512)], ssem.at[2])
    got(fbuf.at[tp, pl.ds(0, 2)], ssem.at[3])
    got(zsend.at[pl.ds(0, NZ - 1)], ssem.at[4])

    @pl.when(half == tp)
    def _():
        got(nrecv.at[pl.ds(0, 15)], ssem.at[5])

    @pl.when(half != tp)
    def _():
        got(nrecv, ssem.at[5])

    got(srecv.at[pl.ds(0, 3)], ssem.at[5])
    got(rrecv.at[pl.ds(0, 3)], ssem.at[6])
    got(fbuf.at[tp], ssem.at[7])
    got(xrecv.at[pl.ds(0, 3)], ssem.at[8])
    got(fbuf.at[tp, y], ssem.at[9])
    got(column(y, pl.ds(0, 3)), ssem.at[10])
    got(column(y, every), ssem.at[11])
    got(column(y, every), ssem.at[11])
    got(my_lanes, ssem.at[12])
    got(dsend.at[pl.ds(0, NZ - 1)], ssem.at[13])
    got(ysend.at[pl.ds(0, 7)], ssem.at[14])


def finish(
    vec_hbm, early_hbm, state_hbm, out_hbm, state_out, st, vec, ob, vt, load_sem, store_sem, small
):
    pairs = [(i, h) for i in range(3) for h in range(4)]
    first = pltpu.make_async_copy(vec_hbm, vec, small.at[0])
    early = pltpu.make_async_copy(early_hbm, ob, small.at[1])
    late = pltpu.make_async_copy(ob, out_hbm, small.at[2])
    loads = [
        pltpu.make_async_copy(state_hbm.at[i, h], st.at[i, h], load_sem.at[i, h]) for i, h in pairs
    ]
    stores = [
        pltpu.make_async_copy(st.at[i, h], state_out.at[i, h], store_sem.at[i, h]) for i, h in pairs
    ]
    for c in [first, early] + loads:
        c.start()
    first.wait()
    vt[...] = jnp.concatenate([vec[0:16, :], jnp.zeros((112, 128), F32)], axis=0).T
    for n, (i, h) in enumerate(pairs):
        r = h * 3 + i
        loads[n].wait()
        kept = st[i, h] * vec[24 + r : 25 + r, :]
        st[i, h] = kept + vt[:, r : r + 1] * vec[12 + r : 13 + r, :]
        stores[n].start()
    early.wait()
    late.start()
    for c in stores + [late]:
        c.wait()


def local_step(
    tokens,
    state,
    mix_gain,
    w_query,
    w_key,
    w_value,
    w_beta,
    w_decay,
    decay_log,
    head_gain,
    w_out,
    ff_gain,
    w_up,
    w_down,
):
    anywhere = pl.BlockSpec(memory_space=pltpu.HBM)
    vmem = pl.BlockSpec(memory_space=pltpu.VMEM)
    early, vec = pl.pallas_call(
        body,
        name="layer",
        out_shape=(
            jax.ShapeDtypeStruct((16, 192), BF16),
            jax.ShapeDtypeStruct((40, 128), F32),
        ),
        in_specs=[anywhere] * 14,
        out_specs=(vmem, vmem),
        scratch_shapes=[
            pltpu.VMEM((16, 192), BF16),
            pltpu.VMEM((1, 16), BF16),
            pltpu.VMEM((1, 16), BF16),
            pltpu.VMEM((4, 32), BF16),
            pltpu.VMEM((4, 32), BF16),
            pltpu.VMEM((1, 128), BF16),
            pltpu.VMEM((1, 4), F32),
            pltpu.VMEM((8, 16, 256), BF16),
            pltpu.VMEM((NY, 3, 32, 512), BF16),
            pltpu.VMEM((4, 128, 1024), BF16),
            pltpu.VMEM((2, NY, 2, 64, D), BF16),
            pltpu.VMEM((3, 4, 128, 128), F32),
            pltpu.VMEM((1024, 256), BF16),
            pltpu.VMEM((1024, 128), BF16),
            pltpu.VMEM((56, 128), F32),
            pltpu.VMEM((NZ * R1, 128), F32),
            pltpu.VMEM((NZ, R1, 128), BF16),
            pltpu.VMEM((NZ, R1, 128), BF16),
            pltpu.VMEM((R1, 128), F32),
            pltpu.VMEM((24, 128), F32),
            pltpu.VMEM((16, 128), F32),
            pltpu.VMEM((16, 128), BF16),
            pltpu.VMEM((16, 16, 128), BF16),
            pltpu.VMEM((256, 128), F32),
            pltpu.VMEM((4, 32, 128), BF16),
            pltpu.VMEM((4, 4, 24, 128), BF16),
            pltpu.VMEM((4, 8, 128), BF16),
            pltpu.VMEM((24, D), BF16),
            pltpu.VMEM((24, 128), F32),
            pltpu.VMEM((NZ, 24, 128), BF16),
            pltpu.VMEM((NZ, 24, 128), BF16),
            pltpu.VMEM((8, 16, 128), BF16),
            pltpu.VMEM((8, 16, 128), BF16),
            pltpu.SemaphoreType.DMA((14,)),
            pltpu.SemaphoreType.DMA((15,)),
            pltpu.SemaphoreType.DMA((15,)),
            pltpu.SemaphoreType.DMA((19,)),
            pltpu.SemaphoreType.REGULAR,
            pltpu.SemaphoreType.REGULAR,
            pltpu.SemaphoreType.REGULAR,
        ],
        compiler_params=pltpu.CompilerParams(
            collective_id=0, has_side_effects=True, vmem_limit_bytes=67043328
        ),
    )(
        tokens.T,
        mix_gain[None, :],
        ff_gain[None, :],
        w_beta.T,
        w_decay.T,
        head_gain[None, :],
        decay_log[None, :],
        state,
        w_query,
        w_key,
        w_value,
        w_out.T,
        w_up.T,
        w_down,
    )
    out, new_state = pl.pallas_call(
        finish,
        name="finish",
        out_shape=(
            jax.ShapeDtypeStruct((16, 192), BF16),
            jax.ShapeDtypeStruct(state.shape, F32),
        ),
        in_specs=[anywhere] * 3,
        out_specs=(anywhere, anywhere),
        scratch_shapes=[
            pltpu.VMEM((3, 4, 128, 128), F32),
            pltpu.VMEM((40, 128), F32),
            pltpu.VMEM((16, 192), BF16),
            pltpu.VMEM((128, 128), F32),
            pltpu.SemaphoreType.DMA((3, 4)),
            pltpu.SemaphoreType.DMA((3, 4)),
            pltpu.SemaphoreType.DMA((3,)),
        ],
        compiler_params=pltpu.CompilerParams(vmem_limit_bytes=67043328),
    )(vec, early, state)
    return out.T, new_state


def solution(mesh):
    placed = (
        P("dp", ("kv", "tp")),
        P(("dp", "kv"), "tp", None, None),
        P(("kv", "tp")),
        P("kv", "tp"),
        P("kv", "tp"),
        P("kv", "tp"),
        P("kv", "tp"),
        P("kv", "tp"),
        P("tp"),
        P(),
        P("tp", "kv"),
        P(("kv", "tp")),
        P(None, ("kv", "tp")),
        P(("kv", "tp"), None),
    )
    return jax.shard_map(
        local_step,
        mesh=mesh,
        in_specs=placed,
        out_specs=(P("dp", ("kv", "tp")), P(("dp", "kv"), "tp", None, None)),
        check_vma=False,
    )
```

time: 66.8 us -> 65.6 us (0.982)
  Pallas kernels: 66 us -> 64.8 us
    pallas_call x1, Pallas kernels: 62.5 us -> 61.7 us  [local_step(): pl.pallas_call(body, name='layer', out_shape=(jax.ShapeDtypeStruct((16, 1...]
where the time goes in v3:
time: 65.6 us; the launch traced here: 65.4 us
  Pallas kernels  64.8 us (99%)
    pallas_call x1, Pallas kernels, local_step(): pl.pallas_call(body, name='layer', out_shape=(jax.ShapeDtypeStruct((16, 1...  61.7 us
    pallas_call x1, Pallas kernels, local_step(): pl.pallas_call(finish, name='finish', out_shape=(jax.ShapeDtypeStruct((16...  3.04 us

profile of v3, /device:TPU:1, one launch (start us, length us, event | category | flops | bytes accessed | tf_op | source)
XLA Modules:
  0.0 65.4 jit_solution(251690961519908951)
XLA Ops:
  0.6 61.7 %layer.1 = (bf16[16,192]{1,0:T(8,128)(2,1)}, f32[40,128]{1,0:T(8,128)}) custom-call(bf16[16,192]{1,0:T(8,128)(2,1)} %bitcast.12, bf16[1,16]{1,0:T(2,128)(2,1)} %bitcast.15, bf16[1,16]{1,0:T(2,128)(2,1)} %bitcast.16, bf16[4,32]{1,0:T(4,128)(2,1)} %bitcast.13, bf16[4,32]{1,0:T(4,128)(2,1)} %bitcast.14, bf16[1,128]{1,0:T(2,128)(2,1)} %bitcast.17, ...), custom_call_target="tpu_custom_call" | custom-call | tf_op jit(solution)/shard_map/layer/pallas_call | solution.py:554
  62.4 3.0 %finish.1 = (bf16[16,192]{1,0:T(8,128)(2,1)}, f32[3,4,128,128]{3,2,1,0:T(8,128)}) custom-call(f32[40,128]{1,0:T(8,128)} %get-tuple-element.6.vec_hbm, bf16[16,192]{1,0:T(8,128)(2,1)} %get-tuple-element.7.early_hbm, f32[3,4,128,128]{3,2,1,0:T(8,128)} %state_hbm.3), custom_call_target="tpu_custom_call" | custom-call | tf_op jit(solution)/shard_map/finish/pallas_call | solution.py:624

commit v4 on v3

--- a/solution.py
+++ b/solution.py
@@ -16,6 +16,7 @@
 NT = (((1,), (1,)), ((), ()))
 R1 = 40
 GATE_AT = 200
+VMEM = 60 * 1024 * 1024
 
 
 def iota(shape, dim):
@@ -38,7 +39,7 @@
     wu_hbm,
     wd_hbm,
     out_ref,
-    vec_ref,
+    state_out,
     tok,
     mixg,
     ffg,
@@ -63,10 +64,8 @@
     nsend,
     nrecv,
     nf,
-    xrecv,
+    rsend,
     rrecv,
-    srecv,
-    xw,
     res,
     dsend,
     drecv,
@@ -92,12 +91,9 @@
     def local(src, dst, k):
         return pltpu.make_async_copy(src, dst, lsem.at[k])
 
-    def mine(block):
-        return wo.at[
-            block,
-            pl.ds(pl.multiple_of(y * 32, 32), 32),
-            pl.ds(pl.multiple_of(tp * 512, 512), 512),
-        ]
+    mine = wo.at[
+        pl.ds(pl.multiple_of(y * 32, 32), 32), pl.ds(pl.multiple_of(tp * 512, 512), 512)
+    ]
 
     loads = [
         local(wq_hbm, wbuf.at[y, 0], 5),
@@ -108,14 +104,14 @@
         local(ff_gain_hbm, ffg, 2),
         local(beta_hbm, bta, 3),
         local(decay_hbm, dcy, 4),
-        local(wo_hbm, mine(0), 8),
+        local(wo_hbm, mine, 8),
         local(wu_hbm, fbuf.at[tp, y, 0], 9),
         local(wd_hbm, fbuf.at[tp, y, 1], 10),
         local(head_gain_hbm, hgain, 11),
         local(decay_log_hbm, dlog, 12),
         local(state_hbm, st, 13),
     ]
-    for c in loads:
+    for c in loads[:3]:
         c.start()
 
     def greet(sem, where):
@@ -124,19 +120,22 @@
     def on_ring(d):
         return {"kv": ((z + d) % NZ) * NY + y}
 
-    def greet_eight(j, carry):
-        p = (me8 + j) % 8
-        greet(barrier, {"kv": z * NY + p // 2, "tp": p % 2})
-        return carry
-
-    lax.fori_loop(1, 8, greet_eight, 0)
-    greet(barrier, on_ring(1))
-    greet(barrier, on_ring(NZ - 1))
+    def at_y(other):
+        return {"kv": z * NY + other}
+
+    above, below, across = (y + 1) % NY, (y + NY - 1) % NY, (y + 2) % NY
+    sibling = {"tp": 1 - tp}
+    beside = [at_y(above), at_y(below), on_ring(1), on_ring(NZ - 1)]
+    diagonal = [{**at_y(above), **sibling}, {**at_y(below), **sibling}]
+    for where in beside + [sibling] + diagonal:
+        greet(barrier, where)
+    for c in loads[3:]:
+        c.start()
 
     for c in loads[:3]:
         c.wait()
 
-    pl.semaphore_wait(barrier, 9)
+    pl.semaphore_wait(barrier, 7)
 
     def push(src, dst, k, where, to=None):
         pltpu.make_async_remote_copy(
@@ -156,13 +155,6 @@
 
         lax.fori_loop(1, 8, one, 0)
 
-    above, below, across = (y + 1) % NY, (y + NY - 1) % NY, (y + 2) % NY
-
-    sibling = {"tp": 1 - tp}
-
-    def at_y(other):
-        return {"kv": z * NY + other}
-
     def got(ref, sem):
         pltpu.make_async_copy(ref, ref, sem).wait()
 
@@ -171,8 +163,8 @@
         push(wbuf.at[y, :, part], wbuf.at[y, :, part], 1, at_y(above), fsem.at[k])
     for part, k in ((low, 2), (high, 3)):
         push(wbuf.at[y, :, part], wbuf.at[y, :, part], 1, at_y(below), fsem.at[k])
-    greet(near_sem, on_ring(1))
-    greet(near_sem, on_ring(NZ - 1))
+    for where in beside:
+        greet(near_sem, where)
 
     row, col = iota((56, 256), 0), iota((56, 256), 1)
     wanted = jnp.where(row < 48, 12 * (row % 16) + 3 * y + row // 16, row + 144)
@@ -195,41 +187,34 @@
     tile = jnp.where(lanes == 192, upright(mixg), jnp.where(lanes == 193, upright(ffg), tile))
     tile = tile + jnp.concatenate([tok[...].astype(F32), jnp.zeros((16, 64), F32)], axis=1)
     tbuf[me8] = tile.astype(BF16)
-    to_eight(lambda p: tbuf.at[me8], tbuf.at[me8], 0)
-    pl.semaphore_wait(near_sem, 2)
+    pl.semaphore_wait(near_sem, 4)
     greet(mid_sem, on_ring(2))
     greet(mid_sem, on_ring(NZ - 2))
-    er, ec = iota((1024, 128), 0), iota((1024, 128), 1)
-    into = er % 256 - GATE_AT
-    spread = jnp.where((ec == er // 256 * 32 + into) & (into >= 0) & (into < 32), 1.0, 0.0)
-    ebuf[...] = spread.astype(BF16)
+    to_eight(lambda p: tbuf.at[me8], tbuf.at[me8], 0)
+    got(wbuf.at[y, :, high], fsem.at[0])
+    push(wbuf.at[below, :, high], wbuf.at[below, :, high], 2, at_y(above), fsem.at[4])
+    got(wbuf.at[y, :, low], fsem.at[2])
+    push(wbuf.at[above, :, low], wbuf.at[above, :, low], 2, at_y(below), fsem.at[5])
     pl.semaphore_wait(mid_sem, 2)
     greet(far_sem, on_ring(4))
     greet(far_sem, on_ring(NZ - 4))
     for c in loads[8:11]:
         c.wait()
-    push(mine(0), mine(3), 10, on_ring(4))
-    push(mine(0), mine(1), 10, on_ring(NZ - 4))
-    got(wbuf.at[y, :, high], fsem.at[0])
-    push(wbuf.at[below, :, high], wbuf.at[below, :, high], 2, at_y(above), fsem.at[4])
-    got(wbuf.at[y, :, low], fsem.at[2])
-    push(wbuf.at[above, :, low], wbuf.at[above, :, low], 2, at_y(below), fsem.at[5])
-    for other, k in ((above, 6), (below, 7)):
-        push(fbuf.at[tp, y, 0], fbuf.at[tp, y, 0], 3, at_y(other), fsem.at[k])
+    for other in (above, below, across):
+        push(mine, mine, 11, at_y(other), fsem.at[8])
+    for m, (a, b) in ((0, (6, 7)), (1, (10, 11))):
+        push(fbuf.at[tp, y, m], fbuf.at[tp, y, m], 3, at_y(above), fsem.at[a])
+        push(fbuf.at[tp, y, m], fbuf.at[tp, y, m], 3, at_y(below), fsem.at[b])
     push(fbuf.at[tp, y], fbuf.at[tp, y], 7, sibling, fsem.at[12])
-    pl.semaphore_wait(far_sem, 2)
-    push(mine(0), mine(2), 10, on_ring(8))
+    er, ec = iota((1024, 128), 0), iota((1024, 128), 1)
+    into = er % 256 - GATE_AT
+    spread = jnp.where((ec == er // 256 * 32 + into) & (into >= 0) & (into < 32), 1.0, 0.0)
+    ebuf[...] = spread.astype(BF16)
     got(tbuf.at[pl.ds(0, 7)], rsem.at[0])
     tiles = tbuf[...]
     turned = tiles.reshape(128, 256)
     chosen = lax.dot_general(pick, turned, NT, preferred_element_type=F32)
     xs[...] = chosen
-    gain_rows = jnp.where(iota((8, 128), 0) == 0, chosen[49:50], 0.0)
-    token_rows = [xs[pl.ds(pl.multiple_of(i * 16 + tp * 8, 8), 8), :] for i in range(3)]
-    xrecv[0] = jnp.concatenate(token_rows + [gain_rows], axis=0).astype(BF16)
-    push(xrecv.at[0], xrecv.at[3], 8, on_ring(4))
-    push(xrecv.at[0], xrecv.at[1], 8, on_ring(NZ - 4))
-    push(xrecv.at[0], xrecv.at[2], 8, on_ring(8))
     x = chosen[:48]
     scaled = (x * chosen[48:49]).astype(BF16)
     square = jnp.sum(x * x, axis=1, keepdims=True)
@@ -268,6 +253,7 @@
 
         lax.fori_loop(0, NZ - 1, one, 0)
 
+    pl.semaphore_wait(far_sem, 2)
     along(lambda far: zsend.at[far], zrecv.at[z], 4)
     zrecv[z] = zsend[z]
     for c in loads[11:]:
@@ -276,20 +262,6 @@
     lane = src_row % 128
     place = 12 * ((src_row // 128 % 2) * 8 + lane % 8) + 3 * (src_row // 256) + lane // 8
     qbuf[...] = jnp.where((seq_col == place) & (lane < 24), 1.0, 0.0).astype(BF16)
-
-    def column(other, blocks):
-        return wo.at[
-            blocks,
-            pl.ds(pl.multiple_of(other * 32, 32), 32),
-            pl.ds(pl.multiple_of(tp * 512, 512), 512),
-        ]
-
-    every, first, last = pl.ds(0, 4), pl.ds(0, 2), pl.ds(2, 2)
-    got(column(y, pl.ds(0, 3)), rsem.at[10])
-    for other, k in ((above, 8), (below, 9)):
-        push(column(y, every), column(y, every), 11, at_y(other), fsem.at[k])
-    for other, k in ((above, 10), (below, 11)):
-        push(fbuf.at[tp, y, 1], fbuf.at[tp, y, 1], 3, at_y(other), fsem.at[k])
     got(zrecv.at[pl.ds(0, NZ - 1)], rsem.at[4])
 
     acc = zrecv[0].astype(F32)
@@ -328,10 +300,9 @@
         kept = st[i, h] * keep[r : r + 1, :]
         predicted = jnp.sum(kept * kc, axis=0, keepdims=True)
         change = beta[r : r + 1, :] * (value[r : r + 1, :] - predicted)
-        vec_ref[12 + r : 13 + r, :] = change
-        hs[r : r + 1, :] = jnp.sum((kept + kc * change) * qc, axis=0, keepdims=True)
-    vec_ref[0:12, :] = knorm
-    vec_ref[24:36, :] = jnp.broadcast_to(keep, (12, 128))
+        new = kept + kc * change
+        state_out[i, h] = new
+        hs[r : r + 1, :] = jnp.sum(new * qc, axis=0, keepdims=True)
     heads = hs[...] / jnp.sqrt(jnp.float32(128))
     heads = jnp.where(iota((16, 128), 0) < 12, heads, 0.0)
     normed = (
@@ -360,10 +331,9 @@
         push(nsend, nrecv.at[slot], 5, {"tp": half})
 
     ahead, behind = pl.ds(0, 32), pl.ds(32, 32)
-    got(column(y, every), fsem.at[8])
-    push(column(below, first), column(below, first), 2, at_y(above), fsem.at[13])
-    got(column(y, every), fsem.at[9])
-    push(column(above, last), column(above, last), 2, at_y(below), fsem.at[14])
+    got(wo.at[pl.ds(0, 96), pl.ds(0, 512)], fsem.at[8])
+    my_lanes = wo.at[:, pl.ds(pl.multiple_of(tp * 512, 512), 512)]
+    push(my_lanes, my_lanes, 12, sibling)
     for m, (a, b, c, d) in ((0, (6, 7, 15, 16)), (1, (10, 11, 17, 18))):
         got(fbuf.at[tp, y, m], fsem.at[a])
         push(
@@ -379,10 +349,6 @@
         )
         for other in (above, below):
             push(fbuf.at[tp, other, m], fbuf.at[tp, other, m], 7, sibling, fsem.at[12])
-    got(column(y, first), fsem.at[13])
-    got(column(y, last), fsem.at[14])
-    my_lanes = wo.at[:, :, pl.ds(pl.multiple_of(tp * 512, 512), 512)]
-    push(my_lanes, my_lanes, 12, sibling)
     @pl.when(half == tp)
     def _():
         got(nrecv.at[pl.ds(0, 15)], rsem.at[5])
@@ -392,7 +358,6 @@
         got(nrecv, rsem.at[5])
 
     got(my_lanes, rsem.at[12])
-    got(xrecv.at[pl.ds(0, 3)], rsem.at[8])
     nf[...] = nrecv[...].astype(F32).reshape(256, 128)
     wide = jnp.concatenate(
         [
@@ -404,18 +369,14 @@
         ],
         axis=1,
     ).astype(BF16)
-    spent = jnp.zeros((24, 128), F32)
-    for j in range(4):
-        mixed = lax.dot_general(wide, wo[j], NT, preferred_element_type=F32)
-        known = xrecv[j].astype(F32)
-        resid = (known[:24] + mixed).astype(BF16).astype(F32)
-        if j == 0:
-            res[...] = resid
-        rrecv[0, j] = (resid * known[24:25]).astype(BF16)
-        spent = spent + resid * resid
+    mixed = lax.dot_general(wide, wo[...], NT, preferred_element_type=F32)
+    token_rows = [xs[pl.ds(pl.multiple_of(i * 16 + tp * 8, 8), 8), :] for i in range(3)]
+    resid = (jnp.concatenate(token_rows, axis=0) + mixed).astype(BF16).astype(F32)
+    res[...] = resid
+    scaled2 = (resid * xs[49:50, :]).astype(BF16).astype(F32)
     total = lax.dot_general(
         jnp.ones((8, 128), F32),
-        jnp.concatenate([spent, jnp.zeros((104, 128), F32)], axis=0),
+        jnp.concatenate([resid * resid, jnp.zeros((104, 128), F32)], axis=0),
         NT,
         preferred_element_type=F32,
         precision=lax.Precision.HIGHEST,
@@ -423,30 +384,25 @@
     total_hi = total.astype(BF16).astype(F32)
     r8 = iota((8, 128), 0)
     tail = jnp.where(r8 == 0, total_hi, jnp.where(r8 == 1, total - total_hi, 0.0))
-    srecv[0] = tail.astype(BF16)
-    for slot_at, d in ((3, NZ - 2), (1, NZ - 1), (2, 1)):
-        push(rrecv.at[0], rrecv.at[slot_at], 6, on_ring(d))
-        push(srecv.at[0], srecv.at[slot_at], 5, on_ring(d), rsem.at[7])
+    rsend[...] = jnp.concatenate([scaled2, tail], axis=0).astype(BF16)
+    along(lambda far: rsend, rrecv.at[z], 6)
+    rrecv[z] = rsend[...]
     for m, (a, b) in ((0, (15, 16)), (1, (17, 18))):
         got(fbuf.at[tp, y, m, ahead], fsem.at[a])
         got(fbuf.at[tp, y, m, behind], fsem.at[b])
         push(fbuf.at[tp, across, m], fbuf.at[tp, across, m], 7, sibling, fsem.at[12])
-    got(rrecv.at[pl.ds(0, 3)], rsem.at[6])
-    got(srecv.at[pl.ds(0, 3)], rsem.at[7])
-    for k, off in enumerate((0, 1, NZ - 1, 2)):
-        for j in range(4):
-            at = pl.multiple_of((z + off + 4 * j) % NZ * 128, 128)
-            xw[:, pl.ds(at, 128)] = rrecv[k, j]
-    sums = srecv[0].astype(F32)
-    for k in range(1, 4):
-        sums = sums + srecv[k].astype(F32)
-    squares = sums[0:1] + sums[1:2]
+    got(rrecv.at[pl.ds(0, NZ - 1)], rsem.at[6])
+    rows = jnp.concatenate([rrecv[k] for k in range(NZ)], axis=1)
+    sums = rrecv[0, 16:32, :].astype(F32)
+    for k in range(1, NZ):
+        sums = sums + rrecv[k, 16:32, :].astype(F32)
+    squares = sums[8:9] + sums[9:10]
     scale = lax.rsqrt(squares / D + 1e-06)
-    dr, dc = iota((24, 128), 0), iota((24, 128), 1)
+    dr, dc = iota((32, 128), 0), iota((32, 128), 1)
     scale = jnp.sum(jnp.where(dr == dc, scale, 0.0), axis=1, keepdims=True)
     got(fbuf.at[0], fsem.at[12])
     up_w = fbuf[:, :, 0].reshape(512, D)
-    up = lax.dot_general(xw[...], up_w, NT, preferred_element_type=F32) * scale
+    up = lax.dot_general(rows, up_w, NT, preferred_element_type=F32) * scale
     act = jnp.square(jnp.maximum(up, 0.0)).astype(BF16)
     for group in ((8, 7, 9, 6), (10, 5, 11, 4), (12, 3, 13, 2), (14, 1, 15, 0)):
         away = [(z + d) % NZ for d in group]
@@ -459,7 +415,7 @@
         )
         part = jnp.dot(act, down_w, preferred_element_type=F32).astype(BF16)
         for n, (d, far) in enumerate(zip(group, away)):
-            dsend[far] = part[:, n * 128 : (n + 1) * 128]
+            dsend[far] = part[:24, n * 128 : (n + 1) * 128]
             if d:
                 push(dsend.at[far], drecv.at[z], 13, {"kv": far * NY + y})
     drecv[z] = dsend[z]
@@ -479,7 +435,6 @@
     got(tbuf.at[pl.ds(0, 7)], ssem.at[0])
     got(wbuf.at[pl.ds(0, 2)], ssem.at[1])
     got(wbuf.at[0], ssem.at[2])
-    got(wo.at[pl.ds(0, 2), pl.ds(0, 64), pl.ds(0, 512)], ssem.at[2])
     got(fbuf.at[tp, pl.ds(0, 2)], ssem.at[3])
     got(zsend.at[pl.ds(0, NZ - 1)], ssem.at[4])
 
@@ -491,46 +446,13 @@
     def _():
         got(nrecv, ssem.at[5])
 
-    got(srecv.at[pl.ds(0, 3)], ssem.at[5])
-    got(rrecv.at[pl.ds(0, 3)], ssem.at[6])
+    got(rrecv.at[pl.ds(0, NZ - 1)], ssem.at[6])
     got(fbuf.at[tp], ssem.at[7])
-    got(xrecv.at[pl.ds(0, 3)], ssem.at[8])
     got(fbuf.at[tp, y], ssem.at[9])
-    got(column(y, pl.ds(0, 3)), ssem.at[10])
-    got(column(y, every), ssem.at[11])
-    got(column(y, every), ssem.at[11])
+    got(wo.at[pl.ds(0, 96), pl.ds(0, 512)], ssem.at[11])
     got(my_lanes, ssem.at[12])
     got(dsend.at[pl.ds(0, NZ - 1)], ssem.at[13])
     got(ysend.at[pl.ds(0, 7)], ssem.at[14])
-
-
-def finish(
-    vec_hbm, early_hbm, state_hbm, out_hbm, state_out, st, vec, ob, vt, load_sem, store_sem, small
-):
-    pairs = [(i, h) for i in range(3) for h in range(4)]
-    first = pltpu.make_async_copy(vec_hbm, vec, small.at[0])
-    early = pltpu.make_async_copy(early_hbm, ob, small.at[1])
-    late = pltpu.make_async_copy(ob, out_hbm, small.at[2])
-    loads = [
-        pltpu.make_async_copy(state_hbm.at[i, h], st.at[i, h], load_sem.at[i, h]) for i, h in pairs
-    ]
-    stores = [
-        pltpu.make_async_copy(st.at[i, h], state_out.at[i, h], store_sem.at[i, h]) for i, h in pairs
-    ]
-    for c in [first, early] + loads:
-        c.start()
-    first.wait()
-    vt[...] = jnp.concatenate([vec[0:16, :], jnp.zeros((112, 128), F32)], axis=0).T
-    for n, (i, h) in enumerate(pairs):
-        r = h * 3 + i
-        loads[n].wait()
-        kept = st[i, h] * vec[24 + r : 25 + r, :]
-        st[i, h] = kept + vt[:, r : r + 1] * vec[12 + r : 13 + r, :]
-        stores[n].start()
-    early.wait()
-    late.start()
-    for c in stores + [late]:
-        c.wait()
 
 
 def local_step(
@@ -551,12 +473,12 @@
 ):
     anywhere = pl.BlockSpec(memory_space=pltpu.HBM)
     vmem = pl.BlockSpec(memory_space=pltpu.VMEM)
-    early, vec = pl.pallas_call(
+    out, new_state = pl.pallas_call(
         body,
         name="layer",
         out_shape=(
-            jax.ShapeDtypeStruct((16, 192), BF16),
-            jax.ShapeDtypeStruct((40, 128), F32),
+            pltpu.VMEM((16, 192), BF16),
+            pltpu.VMEM(state.shape, F32),
         ),
         in_specs=[anywhere] * 14,
         out_specs=(vmem, vmem),
@@ -570,7 +492,7 @@
             pltpu.VMEM((1, 4), F32),
             pltpu.VMEM((8, 16, 256), BF16),
             pltpu.VMEM((NY, 3, 32, 512), BF16),
-            pltpu.VMEM((4, 128, 1024), BF16),
+            pltpu.VMEM((128, 1024), BF16),
             pltpu.VMEM((2, NY, 2, 64, D), BF16),
             pltpu.VMEM((3, 4, 128, 128), F32),
             pltpu.VMEM((1024, 256), BF16),
@@ -585,10 +507,8 @@
             pltpu.VMEM((16, 128), BF16),
             pltpu.VMEM((16, 16, 128), BF16),
             pltpu.VMEM((256, 128), F32),
-            pltpu.VMEM((4, 32, 128), BF16),
-            pltpu.VMEM((4, 4, 24, 128), BF16),
-            pltpu.VMEM((4, 8, 128), BF16),
-            pltpu.VMEM((24, D), BF16),
+            pltpu.VMEM((32, 128), BF16),
+            pltpu.VMEM((NZ, 32, 128), BF16),
             pltpu.VMEM((24, 128), F32),
             pltpu.VMEM((NZ, 24, 128), BF16),
             pltpu.VMEM((NZ, 24, 128), BF16),
@@ -603,7 +523,7 @@
             pltpu.SemaphoreType.REGULAR,
         ],
         compiler_params=pltpu.CompilerParams(
-            collective_id=0, has_side_effects=True, vmem_limit_bytes=67043328
+            collective_id=0, has_side_effects=True, vmem_limit_bytes=VMEM
         ),
     )(
         tokens.T,
@@ -621,26 +541,6 @@
         w_up.T,
         w_down,
     )
-    out, new_state = pl.pallas_call(
-        finish,
-        name="finish",
-        out_shape=(
-            jax.ShapeDtypeStruct((16, 192), BF16),
-            jax.ShapeDtypeStruct(state.shape, F32),
-        ),
-        in_specs=[anywhere] * 3,
-        out_specs=(anywhere, anywhere),
-        scratch_shapes=[
-            pltpu.VMEM((3, 4, 128, 128), F32),
-            pltpu.VMEM((40, 128), F32),
-            pltpu.VMEM((16, 192), BF16),
-            pltpu.VMEM((128, 128), F32),
-            pltpu.SemaphoreType.DMA((3, 4)),
-            pltpu.SemaphoreType.DMA((3, 4)),
-            pltpu.SemaphoreType.DMA((3,)),
-        ],
-        compiler_params=pltpu.CompilerParams(vmem_limit_bytes=67043328),
-    )(vec, early, state)
     return out.T, new_state
 
 

time: 65.6 us -> 62.8 us (0.957)
  Pallas kernels: 64.8 us -> 60.6 us
  local copies, waits for them, and re-layouts: 0 us -> 1.48 us
    pallas_call x2 -> x1, Pallas kernels: 64.8 us -> 60.6 us  [local_step(): pl.pallas_call(body, name='layer', out_shape=(pltpu.VMEM((16, 192), BF16)...]
    unnamed x0 -> x2, local copies, waits for them, and re-layouts: none -> 1.48 us
where the time goes in v4:
time: 62.8 us; the launch traced here: 62.7 us
  Pallas kernels  60.6 us (96%)
  local copies, waits for them, and re-layouts  1.48 us (2%)
  between operations  0.64 us (1%)
    pallas_call x1, Pallas kernels, local_step(): pl.pallas_call(body, name='layer', out_shape=(pltpu.VMEM((16, 192), BF16)...  60.6 us
    unnamed x2, local copies, waits for them, and re-layouts  1.48 us

profile of v4, /device:TPU:1, one launch (start us, length us, event | category | flops | bytes accessed | tf_op | source)
XLA Modules:
  0.0 62.7 jit_solution(16328162187271401877)
XLA Ops:
  0.6 60.6 %layer.1 = (bf16[16,192]{1,0:T(8,128)(2,1)S(1)}, f32[3,4,128,128]{3,2,1,0:T(8,128)S(1)}) custom-call(bf16[16,192]{1,0:T(8,128)(2,1)} %bitcast.13, bf16[1,16]{1,0:T(2,128)(2,1)} %bitcast.16, bf16[1,16]{1,0:T(2,128)(2,1)} %bitcast.17, bf16[4,32]{1,0:T(4,128)(2,1)} %bitcast.14, bf16[4,32]{1,0:T(4,128)(2,1)} %bitcast.15, bf16[1,128]{1,0:T(2,128)(2,1)} %bitcast.18, ...), custom_call_target="tpu_custom_call" | custom-call | tf_op jit(solution)/shard_map/layer/pallas_call | solution.py:476
  61.2 0.6 copy.18
  61.8 0.9 %copy.19 = f32[3,4,128,128]{3,2,1,0:T(8,128)} copy(f32[3,4,128,128]{3,2,1,0:T(8,128)S(1)} %get-tuple-element.7) | data formatting | bytes 1572864

commit v5 on v4

--- a/solution.py
+++ b/solution.py
@@ -129,11 +129,34 @@
     diagonal = [{**at_y(above), **sibling}, {**at_y(below), **sibling}]
     for where in beside + [sibling] + diagonal:
         greet(barrier, where)
-    for c in loads[3:]:
+    for c in loads[3:8]:
         c.start()
 
+    row, col = iota((56, 256), 0), iota((56, 256), 1)
+    wanted = jnp.where(row < 48, 12 * (row % 16) + 3 * y + row // 16, row + 144)
+    pick = jnp.where((col == wanted) & (row < 50), 1.0, 0.0).astype(BF16)
+
+    pr, pc = iota((32, 256), 0), iota((32, 256), 1)
+    shift = jnp.where(pc == pr + GATE_AT, 1.0, 0.0).astype(BF16)
+
+    for c in loads[3:8]:
+        c.wait()
+    sr, sc = iota((16, 16), 0), iota((16, 16), 1)
+
+    def upright(ref):
+        return jnp.sum(jnp.where(sr == sc, ref[...].astype(F32), 0.0), axis=1, keepdims=True)
+
+    gate_rows = jnp.concatenate([bta[...].astype(F32), dcy[...].astype(F32)], axis=0)
+    gate_rows = jnp.concatenate([gate_rows, jnp.zeros((8, 32), F32)], axis=0).astype(BF16)
+    lanes = iota((16, 256), 1)
+    tile = jnp.dot(gate_rows, shift, preferred_element_type=F32)
+    tile = jnp.where(lanes == 192, upright(mixg), jnp.where(lanes == 193, upright(ffg), tile))
+    tile = tile + jnp.concatenate([tok[...].astype(F32), jnp.zeros((16, 64), F32)], axis=1)
+    tbuf[me8] = tile.astype(BF16)
     for c in loads[:3]:
         c.wait()
+    for c in loads[8:]:
+        c.start()
 
     pl.semaphore_wait(barrier, 7)
 
@@ -158,39 +181,25 @@
     def got(ref, sem):
         pltpu.make_async_copy(ref, ref, sem).wait()
 
+    shown = tbuf.at[me8]
+    for where in [at_y(above), at_y(below)] + diagonal + [sibling]:
+        push(shown, shown, 0, where)
     high, low = pl.ds(0, 16), pl.ds(16, 16)
-    for part, k in ((high, 0), (low, 1)):
-        push(wbuf.at[y, :, part], wbuf.at[y, :, part], 1, at_y(above), fsem.at[k])
-    for part, k in ((low, 2), (high, 3)):
-        push(wbuf.at[y, :, part], wbuf.at[y, :, part], 1, at_y(below), fsem.at[k])
+
+    def weights(part, where, k):
+        push(wbuf.at[y, :, part], wbuf.at[y, :, part], 1, where, fsem.at[k])
+
+    weights(high, at_y(above), 0)
+    weights(low, at_y(below), 2)
     for where in beside:
         greet(near_sem, where)
-
-    row, col = iota((56, 256), 0), iota((56, 256), 1)
-    wanted = jnp.where(row < 48, 12 * (row % 16) + 3 * y + row // 16, row + 144)
-    pick = jnp.where((col == wanted) & (row < 50), 1.0, 0.0).astype(BF16)
-
-    pr, pc = iota((32, 256), 0), iota((32, 256), 1)
-    shift = jnp.where(pc == pr + GATE_AT, 1.0, 0.0).astype(BF16)
-
-    for c in loads[3:8]:
-        c.wait()
-    sr, sc = iota((16, 16), 0), iota((16, 16), 1)
-
-    def upright(ref):
-        return jnp.sum(jnp.where(sr == sc, ref[...].astype(F32), 0.0), axis=1, keepdims=True)
-
-    gate_rows = jnp.concatenate([bta[...].astype(F32), dcy[...].astype(F32)], axis=0)
-    gate_rows = jnp.concatenate([gate_rows, jnp.zeros((8, 32), F32)], axis=0).astype(BF16)
-    lanes = iota((16, 256), 1)
-    tile = jnp.dot(gate_rows, shift, preferred_element_type=F32)
-    tile = jnp.where(lanes == 192, upright(mixg), jnp.where(lanes == 193, upright(ffg), tile))
-    tile = tile + jnp.concatenate([tok[...].astype(F32), jnp.zeros((16, 64), F32)], axis=1)
-    tbuf[me8] = tile.astype(BF16)
     pl.semaphore_wait(near_sem, 4)
+    push(shown, shown, 0, at_y(across))
+    push(shown, shown, 0, {**at_y(across), **sibling})
+    weights(low, at_y(above), 1)
+    weights(high, at_y(below), 3)
     greet(mid_sem, on_ring(2))
     greet(mid_sem, on_ring(NZ - 2))
-    to_eight(lambda p: tbuf.at[me8], tbuf.at[me8], 0)
     got(wbuf.at[y, :, high], fsem.at[0])
     push(wbuf.at[below, :, high], wbuf.at[below, :, high], 2, at_y(above), fsem.at[4])
     got(wbuf.at[y, :, low], fsem.at[2])
@@ -241,17 +250,17 @@
                 ]
     for i in range(3):
         zs[pl.ds(36 + i, NZ, R1), :] = gate[i * 16 : (i + 1) * 16]
-    zs[pl.ds(39, NZ, R1), :] = jnp.zeros((NZ, 128), F32)
+    zs[pl.ds(39, NZ, R1), :] = jnp.broadcast_to(chosen[49:50], (NZ, 128))
     zsend[...] = zs[...].reshape(NZ, R1, 128).astype(BF16)
 
-    def along(src_of, dst, k):
+    def along(src_of, dst, k, lower=0, upper=NZ - 1):
         def one(n, carry):
             d = NZ // 2 + ((n + 1) // 2) * (1 - 2 * (n % 2))
             far = (z + d) % NZ
             push(src_of(far), dst, k, {"kv": far * NY + y})
             return carry
 
-        lax.fori_loop(0, NZ - 1, one, 0)
+        lax.fori_loop(lower, upper, one, 0)
 
     pl.semaphore_wait(far_sem, 2)
     along(lambda far: zsend.at[far], zrecv.at[z], 4)
@@ -284,11 +293,13 @@
     lr, lc = iota((12, 4), 0), iota((12, 4), 1)
     rate = jnp.sum(jnp.where(lc == lr // 3, dlog[...], 0.0), axis=1, keepdims=True)
     keep = jnp.exp(-jnp.exp(rate) * soft)
-    query = inverse * accs[0:12, :]
-    key = inverse * accs[12:24, :]
+    query, key = accs[0:12, :], accs[12:24, :]
     value = inverse * accs[24:36, :]
-    qnorm = query * lax.rsqrt(jnp.sum(query * query, axis=1, keepdims=True) + 1e-06)
-    knorm = key * lax.rsqrt(jnp.sum(key * key, axis=1, keepdims=True) + 1e-06)
+    square_of = inverse * inverse
+    qsum = jnp.sum(query * query, axis=1, keepdims=True)
+    ksum = jnp.sum(key * key, axis=1, keepdims=True)
+    qnorm = query * (inverse * lax.rsqrt(square_of * qsum + 1e-06))
+    knorm = key * (inverse * lax.rsqrt(square_of * ksum + 1e-06))
     pad = jnp.zeros((104, 128), F32)
     g12[0:12, :] = qnorm
     g12[12:24, :] = knorm
@@ -373,36 +384,39 @@
     token_rows = [xs[pl.ds(pl.multiple_of(i * 16 + tp * 8, 8), 8), :] for i in range(3)]
     resid = (jnp.concatenate(token_rows, axis=0) + mixed).astype(BF16).astype(F32)
     res[...] = resid
-    scaled2 = (resid * xs[49:50, :]).astype(BF16).astype(F32)
-    total = lax.dot_general(
-        jnp.ones((8, 128), F32),
-        jnp.concatenate([resid * resid, jnp.zeros((104, 128), F32)], axis=0),
-        NT,
-        preferred_element_type=F32,
-        precision=lax.Precision.HIGHEST,
-    )
-    total_hi = total.astype(BF16).astype(F32)
-    r8 = iota((8, 128), 0)
-    tail = jnp.where(r8 == 0, total_hi, jnp.where(r8 == 1, total - total_hi, 0.0))
-    rsend[...] = jnp.concatenate([scaled2, tail], axis=0).astype(BF16)
-    along(lambda far: rsend, rrecv.at[z], 6)
+    rsend[...] = resid.astype(BF16)
+    along(lambda far: rsend, rrecv.at[z], 6, 0, 5)
+    along(lambda far: rsend, rrecv.at[z], 15, 5, NZ - 1)
     rrecv[z] = rsend[...]
     for m, (a, b) in ((0, (15, 16)), (1, (17, 18))):
         got(fbuf.at[tp, y, m, ahead], fsem.at[a])
         got(fbuf.at[tp, y, m, behind], fsem.at[b])
         push(fbuf.at[tp, across, m], fbuf.at[tp, across, m], 7, sibling, fsem.at[12])
-    got(rrecv.at[pl.ds(0, NZ - 1)], rsem.at[6])
-    rows = jnp.concatenate([rrecv[k] for k in range(NZ)], axis=1)
-    sums = rrecv[0, 16:32, :].astype(F32)
-    for k in range(1, NZ):
-        sums = sums + rrecv[k, 16:32, :].astype(F32)
-    squares = sums[8:9] + sums[9:10]
-    scale = lax.rsqrt(squares / D + 1e-06)
-    dr, dc = iota((32, 128), 0), iota((32, 128), 1)
-    scale = jnp.sum(jnp.where(dr == dc, scale, 0.0), axis=1, keepdims=True)
+    def entered(ds):
+        parts, weights_of, spent = [], [], jnp.zeros((24, 128), F32)
+        for d in ds:
+            k = (z + d) % NZ
+            part = rrecv[k].astype(F32)
+            gain = zrecv[k, 32:40, :].astype(F32)[7:8]
+            parts.append((part * gain).astype(BF16))
+            spent = spent + part * part
+            at = pl.multiple_of(k * 128, 128)
+            weights_of.append(fbuf[:, :, 0, :, pl.ds(at, 128)].reshape(512, 128))
+        up = lax.dot_general(
+            jnp.concatenate(parts, axis=1),
+            jnp.concatenate(weights_of, axis=1),
+            NT,
+            preferred_element_type=F32,
+        )
+        return up, spent
+
+    got(rrecv.at[pl.ds(0, 10)], rsem.at[15])
     got(fbuf.at[0], fsem.at[12])
-    up_w = fbuf[:, :, 0].reshape(512, D)
-    up = lax.dot_general(rows, up_w, NT, preferred_element_type=F32) * scale
+    up_near, spent_near = entered((0, 1, 15, 2, 14, 3, 13, 4, 12, 5, 11))
+    got(rrecv.at[pl.ds(0, 5)], rsem.at[6])
+    up_far, spent_far = entered((6, 10, 7, 9, 8))
+    mean = jnp.sum(spent_near + spent_far, axis=1, keepdims=True) / D
+    up = (up_near + up_far) * lax.rsqrt(mean + 1e-06)
     act = jnp.square(jnp.maximum(up, 0.0)).astype(BF16)
     for group in ((8, 7, 9, 6), (10, 5, 11, 4), (12, 3, 13, 2), (14, 1, 15, 0)):
         away = [(z + d) % NZ for d in group]
@@ -415,7 +429,7 @@
         )
         part = jnp.dot(act, down_w, preferred_element_type=F32).astype(BF16)
         for n, (d, far) in enumerate(zip(group, away)):
-            dsend[far] = part[:24, n * 128 : (n + 1) * 128]
+            dsend[far] = part[:, n * 128 : (n + 1) * 128]
             if d:
                 push(dsend.at[far], drecv.at[z], 13, {"kv": far * NY + y})
     drecv[z] = dsend[z]
@@ -446,7 +460,8 @@
     def _():
         got(nrecv, ssem.at[5])
 
-    got(rrecv.at[pl.ds(0, NZ - 1)], ssem.at[6])
+    got(rrecv.at[pl.ds(0, 5)], ssem.at[6])
+    got(rrecv.at[pl.ds(0, 10)], ssem.at[15])
     got(fbuf.at[tp], ssem.at[7])
     got(fbuf.at[tp, y], ssem.at[9])
     got(wo.at[pl.ds(0, 96), pl.ds(0, 512)], ssem.at[11])
@@ -507,16 +522,16 @@
             pltpu.VMEM((16, 128), BF16),
             pltpu.VMEM((16, 16, 128), BF16),
             pltpu.VMEM((256, 128), F32),
-            pltpu.VMEM((32, 128), BF16),
-            pltpu.VMEM((NZ, 32, 128), BF16),
+            pltpu.VMEM((24, 128), BF16),
+            pltpu.VMEM((NZ, 24, 128), BF16),
             pltpu.VMEM((24, 128), F32),
             pltpu.VMEM((NZ, 24, 128), BF16),
             pltpu.VMEM((NZ, 24, 128), BF16),
             pltpu.VMEM((8, 16, 128), BF16),
             pltpu.VMEM((8, 16, 128), BF16),
             pltpu.SemaphoreType.DMA((14,)),
-            pltpu.SemaphoreType.DMA((15,)),
-            pltpu.SemaphoreType.DMA((15,)),
+            pltpu.SemaphoreType.DMA((16,)),
+            pltpu.SemaphoreType.DMA((16,)),
             pltpu.SemaphoreType.DMA((19,)),
             pltpu.SemaphoreType.REGULAR,
             pltpu.SemaphoreType.REGULAR,

time: 62.8 us -> 61.2 us (0.975)
  Pallas kernels: 60.6 us -> 58.9 us
    pallas_call x1, Pallas kernels: 60.6 us -> 58.9 us  [local_step(): pl.pallas_call(body, name='layer', out_shape=(pltpu.VMEM((16, 192), BF16)...]
where the time goes in v5:
time: 61.2 us; the launch traced here: 61 us
  Pallas kernels  58.9 us (96%)
  local copies, waits for them, and re-layouts  1.48 us (2%)
  between operations  0.64 us (1%)
    pallas_call x1, Pallas kernels, local_step(): pl.pallas_call(body, name='layer', out_shape=(pltpu.VMEM((16, 192), BF16)...  58.9 us
    unnamed x2, local copies, waits for them, and re-layouts  1.48 us

profile of v5, /device:TPU:1, one launch (start us, length us, event | category | flops | bytes accessed | tf_op | source)
XLA Modules:
  0.0 61.0 jit_solution(794317576975409681)
XLA Ops:
  0.6 58.9 %layer.1 = (bf16[16,192]{1,0:T(8,128)(2,1)S(1)}, f32[3,4,128,128]{3,2,1,0:T(8,128)S(1)}) custom-call(bf16[16,192]{1,0:T(8,128)(2,1)} %bitcast.13, bf16[1,16]{1,0:T(2,128)(2,1)} %bitcast.16, bf16[1,16]{1,0:T(2,128)(2,1)} %bitcast.17, bf16[4,32]{1,0:T(4,128)(2,1)} %bitcast.14, bf16[4,32]{1,0:T(4,128)(2,1)} %bitcast.15, bf16[1,128]{1,0:T(2,128)(2,1)} %bitcast.18, ...), custom_call_target="tpu_custom_call" | custom-call | tf_op jit(solution)/shard_map/layer/pallas_call | solution.py:491
  59.5 0.6 copy.18
  60.1 0.9 %copy.19 = f32[3,4,128,128]{3,2,1,0:T(8,128)} copy(f32[3,4,128,128]{3,2,1,0:T(8,128)S(1)} %get-tuple-element.7) | data formatting | bytes 1572864

commit v6 on v5

--- a/solution.py
+++ b/solution.py
@@ -14,7 +14,6 @@
 F32 = jnp.float32
 BF16 = jnp.bfloat16
 NT = (((1,), (1,)), ((), ()))
-R1 = 40
 GATE_AT = 200
 VMEM = 60 * 1024 * 1024
 
@@ -55,10 +54,19 @@
     qbuf,
     ebuf,
     xs,
+    za,
+    asend,
+    arecv,
     zs,
     zsend,
     zrecv,
     accs,
+    keys,
+    kt,
+    us,
+    gates_of,
+    upn,
+    spn,
     g12,
     hs,
     nsend,
@@ -132,27 +140,6 @@
     for c in loads[3:8]:
         c.start()
 
-    row, col = iota((56, 256), 0), iota((56, 256), 1)
-    wanted = jnp.where(row < 48, 12 * (row % 16) + 3 * y + row // 16, row + 144)
-    pick = jnp.where((col == wanted) & (row < 50), 1.0, 0.0).astype(BF16)
-
-    pr, pc = iota((32, 256), 0), iota((32, 256), 1)
-    shift = jnp.where(pc == pr + GATE_AT, 1.0, 0.0).astype(BF16)
-
-    for c in loads[3:8]:
-        c.wait()
-    sr, sc = iota((16, 16), 0), iota((16, 16), 1)
-
-    def upright(ref):
-        return jnp.sum(jnp.where(sr == sc, ref[...].astype(F32), 0.0), axis=1, keepdims=True)
-
-    gate_rows = jnp.concatenate([bta[...].astype(F32), dcy[...].astype(F32)], axis=0)
-    gate_rows = jnp.concatenate([gate_rows, jnp.zeros((8, 32), F32)], axis=0).astype(BF16)
-    lanes = iota((16, 256), 1)
-    tile = jnp.dot(gate_rows, shift, preferred_element_type=F32)
-    tile = jnp.where(lanes == 192, upright(mixg), jnp.where(lanes == 193, upright(ffg), tile))
-    tile = tile + jnp.concatenate([tok[...].astype(F32), jnp.zeros((16, 64), F32)], axis=1)
-    tbuf[me8] = tile.astype(BF16)
     for c in loads[:3]:
         c.wait()
     for c in loads[8:]:
@@ -181,40 +168,63 @@
     def got(ref, sem):
         pltpu.make_async_copy(ref, ref, sem).wait()
 
+    high, low = pl.ds(0, 16), pl.ds(16, 16)
+
+    asks, rest = pl.ds(0, 1), pl.ds(1, 2)
+
+    def weights(cols, part, where, k):
+        shard = wbuf.at[y, cols, part]
+        push(shard, shard, 1, where, fsem.at[k])
+
+    weights(asks, high, at_y(above), 0)
+    weights(asks, low, at_y(below), 2)
+    weights(asks, low, at_y(above), 1)
+    weights(asks, high, at_y(below), 3)
+    weights(rest, high, at_y(above), 13)
+    weights(rest, low, at_y(below), 14)
+    for where in beside:
+        greet(near_sem, where)
+    row, col = iota((56, 256), 0), iota((56, 256), 1)
+    wanted = jnp.where(row < 48, 12 * (row % 16) + 3 * y + row // 16, row + 144)
+    pick = jnp.where((col == wanted) & (row < 50), 1.0, 0.0).astype(BF16)
+
+    pr, pc = iota((32, 256), 0), iota((32, 256), 1)
+    shift = jnp.where(pc == pr + GATE_AT, 1.0, 0.0).astype(BF16)
+
+    for c in loads[3:8]:
+        c.wait()
+    sr, sc = iota((16, 16), 0), iota((16, 16), 1)
+
+    def upright(ref):
+        return jnp.sum(jnp.where(sr == sc, ref[...].astype(F32), 0.0), axis=1, keepdims=True)
+
+    gate_rows = jnp.concatenate([bta[...].astype(F32), dcy[...].astype(F32)], axis=0)
+    gate_rows = jnp.concatenate([gate_rows, jnp.zeros((8, 32), F32)], axis=0).astype(BF16)
+    lanes = iota((16, 256), 1)
+    tile = jnp.dot(gate_rows, shift, preferred_element_type=F32)
+    tile = jnp.where(lanes == 192, upright(mixg), jnp.where(lanes == 193, upright(ffg), tile))
+    tile = tile + jnp.concatenate([tok[...].astype(F32), jnp.zeros((16, 64), F32)], axis=1)
+    tbuf[me8] = tile.astype(BF16)
     shown = tbuf.at[me8]
     for where in [at_y(above), at_y(below)] + diagonal + [sibling]:
         push(shown, shown, 0, where)
-    high, low = pl.ds(0, 16), pl.ds(16, 16)
-
-    def weights(part, where, k):
-        push(wbuf.at[y, :, part], wbuf.at[y, :, part], 1, where, fsem.at[k])
-
-    weights(high, at_y(above), 0)
-    weights(low, at_y(below), 2)
-    for where in beside:
-        greet(near_sem, where)
     pl.semaphore_wait(near_sem, 4)
     push(shown, shown, 0, at_y(across))
     push(shown, shown, 0, {**at_y(across), **sibling})
-    weights(low, at_y(above), 1)
-    weights(high, at_y(below), 3)
+    weights(rest, low, at_y(above), 8)
+    weights(rest, high, at_y(below), 9)
     greet(mid_sem, on_ring(2))
     greet(mid_sem, on_ring(NZ - 2))
-    got(wbuf.at[y, :, high], fsem.at[0])
-    push(wbuf.at[below, :, high], wbuf.at[below, :, high], 2, at_y(above), fsem.at[4])
-    got(wbuf.at[y, :, low], fsem.at[2])
-    push(wbuf.at[above, :, low], wbuf.at[above, :, low], 2, at_y(below), fsem.at[5])
     pl.semaphore_wait(mid_sem, 2)
     greet(far_sem, on_ring(4))
     greet(far_sem, on_ring(NZ - 4))
-    for c in loads[8:11]:
-        c.wait()
-    for other in (above, below, across):
-        push(mine, mine, 11, at_y(other), fsem.at[8])
-    for m, (a, b) in ((0, (6, 7)), (1, (10, 11))):
-        push(fbuf.at[tp, y, m], fbuf.at[tp, y, m], 3, at_y(above), fsem.at[a])
-        push(fbuf.at[tp, y, m], fbuf.at[tp, y, m], 3, at_y(below), fsem.at[b])
-    push(fbuf.at[tp, y], fbuf.at[tp, y], 7, sibling, fsem.at[12])
+    for cols, (a, b, c, d) in ((asks, (0, 2, 4, 5)), (rest, (13, 14, 19, 20))):
+        got(wbuf.at[y, cols, high], fsem.at[a])
+        shard = wbuf.at[below, cols, high]
+        push(shard, shard, 2, at_y(above), fsem.at[c])
+        got(wbuf.at[y, cols, low], fsem.at[b])
+        shard = wbuf.at[above, cols, low]
+        push(shard, shard, 2, at_y(below), fsem.at[d])
     er, ec = iota((1024, 128), 0), iota((1024, 128), 1)
     into = er % 256 - GATE_AT
     spread = jnp.where((ec == er // 256 * 32 + into) & (into >= 0) & (into < 32), 1.0, 0.0)
@@ -236,22 +246,22 @@
     gl = iota((48, 128), 1)
     gate = jnp.where(gl == 8, square_hi, jnp.where(gl == 9, square - square_hi, gate))
 
-    got(wbuf.at[y, :, low], fsem.at[1])
-    got(wbuf.at[y, :, high], fsem.at[3])
-    got(wbuf.at[y, :, high], fsem.at[4])
-    got(wbuf.at[y, :, low], fsem.at[5])
-    for m in range(3):
-        weight = wbuf[:, m].reshape(128, 512)
-        part = jnp.dot(scaled, weight, preferred_element_type=F32)
-        for h in range(4):
-            for i in range(3):
-                zs[pl.ds(m * 12 + h * 3 + i, NZ, R1), :] = part[
-                    i * 16 : (i + 1) * 16, h * 128 : (h + 1) * 128
-                ]
+
+    def complete(cols, ks):
+        for part, k in zip((low, high, high, low), ks):
+            got(wbuf.at[y, cols, part], fsem.at[k])
+
+    complete(asks, (1, 3, 4, 5))
+    part = jnp.dot(scaled, wbuf[:, 0].reshape(128, 512), preferred_element_type=F32)
+    for h in range(4):
+        for i in range(3):
+            za[pl.ds(h * 3 + i, NZ, 16), :] = part[
+                i * 16 : (i + 1) * 16, h * 128 : (h + 1) * 128
+            ]
     for i in range(3):
-        zs[pl.ds(36 + i, NZ, R1), :] = gate[i * 16 : (i + 1) * 16]
-    zs[pl.ds(39, NZ, R1), :] = jnp.broadcast_to(chosen[49:50], (NZ, 128))
-    zsend[...] = zs[...].reshape(NZ, R1, 128).astype(BF16)
+        za[pl.ds(12 + i, NZ, 16), :] = gate[i * 16 : (i + 1) * 16]
+    za[pl.ds(15, NZ, 16), :] = jnp.broadcast_to(chosen[49:50], (NZ, 128))
+    asend[...] = za[...].reshape(NZ, 16, 128).astype(BF16)
 
     def along(src_of, dst, k, lower=0, upper=NZ - 1):
         def one(n, carry):
@@ -263,22 +273,40 @@
         lax.fori_loop(lower, upper, one, 0)
 
     pl.semaphore_wait(far_sem, 2)
-    along(lambda far: zsend.at[far], zrecv.at[z], 4)
+    along(lambda far: asend.at[far], arecv.at[z], 4)
+    complete(rest, (8, 9, 19, 20))
+    for m in range(1, 3):
+        part = jnp.dot(scaled, wbuf[:, m].reshape(128, 512), preferred_element_type=F32)
+        for h in range(4):
+            for i in range(3):
+                zs[pl.ds((m - 1) * 12 + h * 3 + i, NZ, 24), :] = part[
+                    i * 16 : (i + 1) * 16, h * 128 : (h + 1) * 128
+                ]
+    zsend[...] = zs[...].reshape(NZ, 24, 128).astype(BF16)
+    along(lambda far: zsend.at[far], zrecv.at[z], 8)
+    for c in loads[8:11]:
+        c.wait()
+    for other in (above, below, across):
+        push(mine, mine, 11, at_y(other), rsem.at[2])
+    for m, (a, b) in ((0, (6, 7)), (1, (10, 11))):
+        push(fbuf.at[tp, y, m], fbuf.at[tp, y, m], 3, at_y(above), fsem.at[a])
+        push(fbuf.at[tp, y, m], fbuf.at[tp, y, m], 3, at_y(below), fsem.at[b])
+    push(fbuf.at[tp, y], fbuf.at[tp, y], 7, sibling, fsem.at[12])
     zrecv[z] = zsend[z]
+    arecv[z] = asend[z]
     for c in loads[11:]:
         c.wait()
     src_row, seq_col = iota((1024, 256), 0), iota((1024, 256), 1)
     lane = src_row % 128
     place = 12 * ((src_row // 128 % 2) * 8 + lane % 8) + 3 * (src_row // 256) + lane // 8
     qbuf[...] = jnp.where((seq_col == place) & (lane < 24), 1.0, 0.0).astype(BF16)
-    got(zrecv.at[pl.ds(0, NZ - 1)], rsem.at[4])
-
-    acc = zrecv[0].astype(F32)
+    got(arecv.at[pl.ds(0, NZ - 1)], rsem.at[4])
+    acc = arecv[0].astype(F32)
     for k in range(1, NZ):
-        acc = acc + zrecv[k].astype(F32)
-    accs[...] = acc
+        acc = acc + arecv[k].astype(F32)
+    accs[0:16, :] = acc
     for h in range(4):
-        g12[3 * h : 3 * h + 3, :] = accs[36:39, :]
+        g12[3 * h : 3 * h + 3, :] = accs[12:15, :]
     g = g12[0:12, :]
     r12, l12 = iota((12, 128), 0), iota((12, 128), 1)
     head_of = r12 // 3
@@ -293,29 +321,42 @@
     lr, lc = iota((12, 4), 0), iota((12, 4), 1)
     rate = jnp.sum(jnp.where(lc == lr // 3, dlog[...], 0.0), axis=1, keepdims=True)
     keep = jnp.exp(-jnp.exp(rate) * soft)
-    query, key = accs[0:12, :], accs[12:24, :]
-    value = inverse * accs[24:36, :]
     square_of = inverse * inverse
-    qsum = jnp.sum(query * query, axis=1, keepdims=True)
-    ksum = jnp.sum(key * key, axis=1, keepdims=True)
-    qnorm = query * (inverse * lax.rsqrt(square_of * qsum + 1e-06))
-    knorm = key * (inverse * lax.rsqrt(square_of * ksum + 1e-06))
-    pad = jnp.zeros((104, 128), F32)
-    g12[0:12, :] = qnorm
-    g12[12:24, :] = knorm
-    both = jnp.concatenate([g12[...], pad], axis=0).T
+
+    def unit(rows):
+        size = jnp.sum(rows * rows, axis=1, keepdims=True)
+        return rows * (inverse * lax.rsqrt(square_of * size + 1e-06))
+
+    pad = jnp.zeros((112, 128), F32)
+    qnorm = unit(accs[0:12, :])
+    keys[0:12, :] = qnorm
+    keys[12:16, :] = jnp.zeros((4, 128), F32)
+    across_q = jnp.concatenate([keys[...], pad], axis=0).T
     for r in range(12):
         h, i = r // 3, r % 3
-        kc = both[:, 12 + r : 13 + r]
-        qc = both[:, r : r + 1]
         kept = st[i, h] * keep[r : r + 1, :]
-        predicted = jnp.sum(kept * kc, axis=0, keepdims=True)
-        change = beta[r : r + 1, :] * (value[r : r + 1, :] - predicted)
-        new = kept + kc * change
-        state_out[i, h] = new
-        hs[r : r + 1, :] = jnp.sum(new * qc, axis=0, keepdims=True)
-    heads = hs[...] / jnp.sqrt(jnp.float32(128))
-    heads = jnp.where(iota((16, 128), 0) < 12, heads, 0.0)
+        st[i, h] = kept
+        hs[r : r + 1, :] = jnp.sum(kept * across_q[:, r : r + 1], axis=0, keepdims=True)
+    gates_of[:, 0:1] = beta
+    gates_of[:, 1:2] = inverse
+    gates_of[:, 2:3] = square_of
+    got(zrecv.at[pl.ds(0, NZ - 1)], rsem.at[8])
+    acc = zrecv[0].astype(F32)
+    for k in range(1, NZ):
+        acc = acc + zrecv[k].astype(F32)
+    accs[16:40, :] = acc
+    beta, inverse, square_of = gates_of[:, 0:1], gates_of[:, 1:2], gates_of[:, 2:3]
+    knorm = unit(accs[16:28, :])
+    value = inverse * accs[28:40, :]
+    shared = jnp.sum(knorm * keys[0:12, :], axis=1, keepdims=True)
+    keys[0:12, :] = knorm
+    kt[...] = jnp.concatenate([keys[...], pad], axis=0).T
+    for r in range(12):
+        us[r : r + 1, :] = jnp.sum(st[r % 3, r // 3] * kt[:, r : r + 1], axis=0, keepdims=True)
+    change = beta * (value - us[0:12, :])
+    us[0:12, :] = change
+    heads = (hs[0:12, :] + shared * change) / jnp.sqrt(jnp.float32(128))
+    heads = jnp.concatenate([heads, jnp.zeros((4, 128), F32)], axis=0)
     normed = (
         heads
         * lax.rsqrt(jnp.mean(heads * heads, axis=1, keepdims=True) + 1e-06)
@@ -341,8 +382,11 @@
     def _():
         push(nsend, nrecv.at[slot], 5, {"tp": half})
 
+    for r in range(12):
+        h, i = r // 3, r % 3
+        state_out[i, h] = st[i, h] + kt[:, r : r + 1] * us[r : r + 1, :]
     ahead, behind = pl.ds(0, 32), pl.ds(32, 32)
-    got(wo.at[pl.ds(0, 96), pl.ds(0, 512)], fsem.at[8])
+    got(wo.at[pl.ds(0, 96), pl.ds(0, 512)], rsem.at[2])
     my_lanes = wo.at[:, pl.ds(pl.multiple_of(tp * 512, 512), 512)]
     push(my_lanes, my_lanes, 12, sibling)
     for m, (a, b, c, d) in ((0, (6, 7, 15, 16)), (1, (10, 11, 17, 18))):
@@ -385,8 +429,8 @@
     resid = (jnp.concatenate(token_rows, axis=0) + mixed).astype(BF16).astype(F32)
     res[...] = resid
     rsend[...] = resid.astype(BF16)
-    along(lambda far: rsend, rrecv.at[z], 6, 0, 5)
-    along(lambda far: rsend, rrecv.at[z], 15, 5, NZ - 1)
+    along(lambda far: rsend, rrecv.at[z], 6, 0, 3)
+    along(lambda far: rsend, rrecv.at[z], 15, 3, NZ - 1)
     rrecv[z] = rsend[...]
     for m, (a, b) in ((0, (15, 16)), (1, (17, 18))):
         got(fbuf.at[tp, y, m, ahead], fsem.at[a])
@@ -397,7 +441,7 @@
         for d in ds:
             k = (z + d) % NZ
             part = rrecv[k].astype(F32)
-            gain = zrecv[k, 32:40, :].astype(F32)[7:8]
+            gain = arecv[k].astype(F32)[15:16]
             parts.append((part * gain).astype(BF16))
             spent = spent + part * part
             at = pl.multiple_of(k * 128, 128)
@@ -410,13 +454,15 @@
         )
         return up, spent
 
-    got(rrecv.at[pl.ds(0, 10)], rsem.at[15])
+    got(rrecv.at[pl.ds(0, 12)], rsem.at[15])
     got(fbuf.at[0], fsem.at[12])
-    up_near, spent_near = entered((0, 1, 15, 2, 14, 3, 13, 4, 12, 5, 11))
-    got(rrecv.at[pl.ds(0, 5)], rsem.at[6])
-    up_far, spent_far = entered((6, 10, 7, 9, 8))
-    mean = jnp.sum(spent_near + spent_far, axis=1, keepdims=True) / D
-    up = (up_near + up_far) * lax.rsqrt(mean + 1e-06)
+    up_near, spent_near = entered((0, 1, 15, 2, 14, 3, 13, 4, 12, 5, 11, 6, 10))
+    upn[...] = up_near
+    spn[...] = spent_near
+    got(rrecv.at[pl.ds(0, 3)], rsem.at[6])
+    up_far, spent_far = entered((7, 9, 8))
+    mean = jnp.sum(spn[...] + spent_far, axis=1, keepdims=True) / D
+    up = (upn[...] + up_far) * lax.rsqrt(mean + 1e-06)
     act = jnp.square(jnp.maximum(up, 0.0)).astype(BF16)
     for group in ((8, 7, 9, 6), (10, 5, 11, 4), (12, 3, 13, 2), (14, 1, 15, 0)):
         away = [(z + d) % NZ for d in group]
@@ -450,7 +496,8 @@
     got(wbuf.at[pl.ds(0, 2)], ssem.at[1])
     got(wbuf.at[0], ssem.at[2])
     got(fbuf.at[tp, pl.ds(0, 2)], ssem.at[3])
-    got(zsend.at[pl.ds(0, NZ - 1)], ssem.at[4])
+    got(asend.at[pl.ds(0, NZ - 1)], ssem.at[4])
+    got(zsend.at[pl.ds(0, NZ - 1)], ssem.at[8])
 
     @pl.when(half == tp)
     def _():
@@ -460,14 +507,25 @@
     def _():
         got(nrecv, ssem.at[5])
 
-    got(rrecv.at[pl.ds(0, 5)], ssem.at[6])
-    got(rrecv.at[pl.ds(0, 10)], ssem.at[15])
+    got(rrecv.at[pl.ds(0, 3)], ssem.at[6])
+    got(rrecv.at[pl.ds(0, 12)], ssem.at[15])
     got(fbuf.at[tp], ssem.at[7])
     got(fbuf.at[tp, y], ssem.at[9])
     got(wo.at[pl.ds(0, 96), pl.ds(0, 512)], ssem.at[11])
     got(my_lanes, ssem.at[12])
     got(dsend.at[pl.ds(0, NZ - 1)], ssem.at[13])
     got(ysend.at[pl.ds(0, 7)], ssem.at[14])
+
+
+def leave(early_ref, state_ref, out_hbm, state_hbm, sem):
+    copies = [
+        pltpu.make_async_copy(state_ref, state_hbm, sem.at[0]),
+        pltpu.make_async_copy(early_ref, out_hbm, sem.at[1]),
+    ]
+    for c in copies:
+        c.start()
+    for c in copies:
+        c.wait()
 
 
 def local_step(
@@ -488,7 +546,7 @@
 ):
     anywhere = pl.BlockSpec(memory_space=pltpu.HBM)
     vmem = pl.BlockSpec(memory_space=pltpu.VMEM)
-    out, new_state = pl.pallas_call(
+    early, held = pl.pallas_call(
         body,
         name="layer",
         out_shape=(
@@ -513,10 +571,19 @@
             pltpu.VMEM((1024, 256), BF16),
             pltpu.VMEM((1024, 128), BF16),
             pltpu.VMEM((56, 128), F32),
-            pltpu.VMEM((NZ * R1, 128), F32),
-            pltpu.VMEM((NZ, R1, 128), BF16),
-            pltpu.VMEM((NZ, R1, 128), BF16),
-            pltpu.VMEM((R1, 128), F32),
+            pltpu.VMEM((NZ * 16, 128), F32),
+            pltpu.VMEM((NZ, 16, 128), BF16),
+            pltpu.VMEM((NZ, 16, 128), BF16),
+            pltpu.VMEM((NZ * 24, 128), F32),
+            pltpu.VMEM((NZ, 24, 128), BF16),
+            pltpu.VMEM((NZ, 24, 128), BF16),
+            pltpu.VMEM((40, 128), F32),
+            pltpu.VMEM((16, 128), F32),
+            pltpu.VMEM((128, 128), F32),
+            pltpu.VMEM((16, 128), F32),
+            pltpu.VMEM((12, 128), F32),
+            pltpu.VMEM((24, 512), F32),
+            pltpu.VMEM((24, 128), F32),
             pltpu.VMEM((24, 128), F32),
             pltpu.VMEM((16, 128), F32),
             pltpu.VMEM((16, 128), BF16),
@@ -532,7 +599,7 @@
             pltpu.SemaphoreType.DMA((14,)),
             pltpu.SemaphoreType.DMA((16,)),
             pltpu.SemaphoreType.DMA((16,)),
-            pltpu.SemaphoreType.DMA((19,)),
+            pltpu.SemaphoreType.DMA((21,)),
             pltpu.SemaphoreType.REGULAR,
             pltpu.SemaphoreType.REGULAR,
             pltpu.SemaphoreType.REGULAR,
@@ -556,6 +623,18 @@
         w_up.T,
         w_down,
     )
+    out, new_state = pl.pallas_call(
+        leave,
+        name="leave",
+        out_shape=(
+            jax.ShapeDtypeStruct((16, 192), BF16),
+            jax.ShapeDtypeStruct(state.shape, F32),
+        ),
+        in_specs=[pl.BlockSpec(memory_space=pl.ANY)] * 2,
+        out_specs=(anywhere, anywhere),
+        scratch_shapes=[pltpu.SemaphoreType.DMA((2,))],
+        compiler_params=pltpu.CompilerParams(vmem_limit_bytes=1024 * 1024),
+    )(early, held)
     return out.T, new_state
 
 

time: 61.2 us -> 60.4 us (0.987)
  local copies, waits for them, and re-layouts: 1.48 us -> 0 us
  Pallas kernels: 58.9 us -> 59.6 us
    unnamed x2 -> x0, local copies, waits for them, and re-layouts: 1.48 us -> none
    pallas_call x0 -> x1, Pallas kernels: none -> 0.9 us  [local_step(): pl.pallas_call(leave, name='leave', out_shape=(jax.ShapeDtypeStruct((16,...]
where the time goes in v6:
time: 60.4 us; the launch traced here: 60.3 us
  Pallas kernels  59.6 us (99%)
  between operations  0.64 us (1%)
    pallas_call x1, Pallas kernels, local_step(): pl.pallas_call(body, name='layer', out_shape=(pltpu.VMEM((16, 192), BF16)...  58.7 us

profile of v6, /device:TPU:1, one launch (start us, length us, event | category | flops | bytes accessed | tf_op | source)
XLA Modules:
  0.0 60.3 jit_solution(10192704649734963382)
XLA Ops:
  0.6 58.7 %layer.1 = (bf16[16,192]{1,0:T(8,128)(2,1)S(1)}, f32[3,4,128,128]{3,2,1,0:T(8,128)S(1)}) custom-call(bf16[16,192]{1,0:T(8,128)(2,1)} %bitcast.12, bf16[1,16]{1,0:T(2,128)(2,1)} %bitcast.15, bf16[1,16]{1,0:T(2,128)(2,1)} %bitcast.16, bf16[4,32]{1,0:T(4,128)(2,1)} %bitcast.13, bf16[4,32]{1,0:T(4,128)(2,1)} %bitcast.14, bf16[1,128]{1,0:T(2,128)(2,1)} %bitcast.17, ...), custom_call_target="tpu_custom_call" | custom-call | tf_op jit(solution)/shard_map/layer/pallas_call | solution.py:549
  59.4 0.9 %leave.1 = (bf16[16,192]{1,0:T(8,128)(2,1)}, f32[3,4,128,128]{3,2,1,0:T(8,128)}) custom-call(bf16[16,192]{1,0:T(8,128)(2,1)S(1)} %get-tuple-element.6.early_ref, f32[3,4,128,128]{3,2,1,0:T(8,128)S(1)} %get-tuple-element.7.state_ref), custom_call_target="tpu_custom_call" | custom-call | tf_op jit(solution)/shard_map/leave/pallas_call | solution.py:626
